TPU v7x, 256 devices: a whole 4x4x8 slice. The times are simulated.
256 devices in a mesh: sp: 64 (over z, x, core), tp: 4 (over y).
Axes of the slice: x: 4, y: 4, z: 8, core: 2. Of those that a mesh axis runs over, the one named last changes fastest.
Arguments:
- tokens: bfloat16 [16384, 2048], P('sp', 'tp'), may hold values from -6 to 6
- norm_gain: float32 [2048], replicated, may hold values from 0.1 to 1.9
- query_one: bfloat16 [2048, 512], P('sp', 'tp'), may hold values from -1 to 1
- key_one: bfloat16 [2048, 512], P('sp', 'tp'), may hold values from -1 to 1
- query_two: bfloat16 [2048, 512], P('sp', 'tp'), may hold values from -0.15625 to 0.15625
- key_two: bfloat16 [2048, 512], P('sp', 'tp'), may hold values from -0.15625 to 0.15625
- value_weight: bfloat16 [2048, 1024], P('sp', 'tp'), may hold values from -0.5 to 0.5
- pool_weight: bfloat16 [2048, 1024], P('sp', 'tp'), may hold values from -0.125 to 0.125
- lambda_head: float32 [8], replicated, may hold values from 0.3 to 0.8
- head_gain: float32 [128], replicated, may hold values from 0.1 to 1.9
- group_weight: bfloat16 [8, 128, 128], replicated, may hold values from -0.5 to 0.5
- pool_scale: float32 [1024], replicated, may hold values from 0.1 to 1.9
- out_attn: bfloat16 [1024, 2048], P('tp', 'sp'), may hold values from -0.125 to 0.125
- out_pool: bfloat16 [1024, 2048], P('tp', 'sp'), may hold values from -0.125 to 0.125
Outputs:
- mixed: bfloat16 [16384, 2048], P(('sp', 'tp'))
All inputs are finite; a program needn't handle non-finite values.
Results may differ from a plain program's by a relative error of at most 0.013.
Values may be sent and summed in bfloat16 or wider, within the bound.
A program may use at most 128 MiB of HBM per device.

v0:
```python
import math

import jax
import jax.numpy as jnp
from jax import lax
from jax.sharding import PartitionSpec as P

HEAD_DIM = 64
VALUE_DIM = 128
GROUP_DIM = 128


rope_base = 500000.0
head_scale = 0.8
norm_floor = 1e-06
head_floor = 0.001
masked_score = -1e30
pool_reach = 15
key_block = 1024


def joined_along(blocks, dim):
    lengths = list(blocks.shape[1:])
    lengths[dim] *= blocks.shape[0]
    return jnp.moveaxis(blocks, 0, dim).reshape(lengths)


def from_everyone(x, axis):
    peers = lax.axis_size(axis)
    return lax.all_to_all(jnp.broadcast_to(x[None], (peers, *x.shape)), axis, 0, 0, tiled=True)


def gathered_copies(x, axis, dim):
    return joined_along(from_everyone(x, axis), dim)


def side_by_side(arrays, axis, dim, along):
    widths = [a.shape[along] for a in arrays]
    both = jnp.concatenate(arrays, axis=along)
    out = lax.all_gather(both, axis, axis=dim, tiled=True)
    return tuple(jnp.split(out, [sum(widths[:k]) for k in range(1, len(widths))], axis=along))


def from_behind(x, axis, by):
    peers = lax.axis_size(axis)
    pairs = [(i, i + by) for i in range(peers) if 0 <= i + by < peers]
    return lax.ppermute(x, axis, pairs)


def rows_first(arrays, axis, dims):
    turned = [jnp.moveaxis(a, dim, 0) for a, dim in zip(arrays, dims)]
    widths = [t[0].size for t in turned]
    both = jnp.concatenate([t.reshape(-1, w) for t, w in zip(turned, widths)], axis=1)
    out = lax.all_gather(both, axis, axis=0, tiled=True)
    blocks = jnp.split(out, [sum(widths[:k]) for k in range(1, len(widths))], axis=1)
    return tuple(
        (
            jnp.moveaxis(b.reshape(-1, *t.shape[1:]), 0, dim)
            for b, t, dim in zip(blocks, turned, dims)
        )
    )


def in_blocks(x, dim, peers):
    before, after = (x.shape[:dim], x.shape[dim + 1 :])
    return jnp.moveaxis(x.reshape(*before, peers, -1, *after), dim, 0)


def sum_at_owner(x, axis, dim):
    peers = lax.axis_size(axis)
    blocks = lax.all_to_all(in_blocks(x, dim, peers), axis, 0, 0, tiled=True)
    return jnp.sum(blocks.astype(jnp.float32), axis=0)


def rotate(values_in, positions):
    half_dim = values_in.shape[-1] // 2
    inverse = rope_base ** (-(jnp.arange(half_dim, dtype=jnp.float32) * 2.0 / values_in.shape[-1]))
    angles = positions.astype(jnp.float32)[:, None] * inverse[None, :]
    cosine = jnp.cos(angles)[:, None, :]
    sine_part = jnp.sin(angles)[:, None, :]
    first_half = values_in[..., :half_dim]
    second_half = values_in[..., half_dim:]
    return jnp.concatenate(
        [
            first_half * cosine - second_half * sine_part,
            second_half * cosine + first_half * sine_part,
        ],
        axis=-1,
    )


def body(
    tokens,
    norm_gain,
    query_one,
    key_one,
    query_two,
    key_two,
    value_weight,
    pool_weight,
    lambda_head,
    head_gain,
    group_weight,
    pool_scale,
    out_attn,
    out_pool,
):
    tok_rows = tokens.shape[0]
    local_heads = query_one.shape[1] // HEAD_DIM
    local_groups = pool_weight.shape[1] // GROUP_DIM
    tp_index = lax.axis_index("tp")
    positions = lax.axis_index("sp") * tok_rows + jnp.arange(tok_rows, dtype=jnp.int32)
    score_scale = HEAD_DIM ** (-0.5)
    gathered = gathered_copies(tokens, "tp", 1)
    float_rows = gathered.astype(jnp.float32)
    normed = (
        float_rows
        * lax.rsqrt(jnp.mean(float_rows * float_rows, axis=-1, keepdims=True) + norm_floor)
        * norm_gain
    ).astype(jnp.bfloat16)

    def contract(shard_part):
        return jnp.dot(normed, shard_part, preferred_element_type=jnp.float32)

    pieces = side_by_side(
        (query_one, key_one, query_two, key_two, value_weight, pool_weight), "sp", 0, 1
    )
    everything = tuple((contract(shard_part) for shard_part in pieces))
    projected = everything[:5]
    pool_proj = everything[5]

    def turned(flat_part):
        return rotate(flat_part.reshape(tok_rows, local_heads, HEAD_DIM), positions).astype(
            jnp.bfloat16
        )

    query_a = turned(projected[0])
    key_a = turned(projected[1]).reshape(tok_rows, local_heads * HEAD_DIM)
    query_b = turned(projected[2])
    key_b = turned(projected[3]).reshape(tok_rows, local_heads * HEAD_DIM)
    value_rows = projected[4].astype(jnp.bfloat16)
    queries = (query_a, query_b)
    initial = (
        jnp.full((2, tok_rows, local_heads), masked_score, jnp.float32),
        jnp.zeros((2, tok_rows, local_heads), jnp.float32),
        jnp.zeros((2, tok_rows, local_heads, VALUE_DIM), jnp.float32),
    )
    pieces = side_by_side((key_a, key_b, value_rows), "sp", 0, 1)
    key_rows = pieces[0].shape[0]
    key_span = math.gcd(key_rows, key_block)
    count_blocks = key_rows // key_span
    stacked = tuple((member.reshape(count_blocks, key_span, local_heads, -1) for member in pieces))

    def step_block(carried, inputs):
        maxima, totals, accums = carried
        block_a, block_b, block_v, block_id = inputs
        key_pos = block_id * key_span + jnp.arange(key_span, dtype=jnp.int32)
        visible = (key_pos[None, :] <= positions[:, None])[:, None, :]
        new_maxima, new_totals, new_accums = ([], [], [])
        for map_index, key_part in enumerate((block_a, block_b)):
            scores = (
                jnp.einsum(
                    "qhd,khd->qhk", queries[map_index], key_part, preferred_element_type=jnp.float32
                )
                * score_scale
            )
            scores = jnp.where(visible, scores, masked_score)
            top_now = jnp.maximum(maxima[map_index], jnp.max(scores, axis=-1))
            factor = jnp.exp(maxima[map_index] - top_now)
            weights = jnp.where(visible, jnp.exp(scores - top_now[..., None]), 0.0)
            new_maxima.append(top_now)
            new_totals.append(totals[map_index] * factor + jnp.sum(weights, axis=-1))
            product = jnp.einsum(
                "qhk,khd->qhd",
                weights.astype(jnp.bfloat16),
                block_v,
                preferred_element_type=jnp.float32,
            )
            new_accums.append(accums[map_index] * factor[..., None] + product)
        return ((jnp.stack(new_maxima), jnp.stack(new_totals), jnp.stack(new_accums)), None)

    result_state, _ = lax.scan(
        step_block,
        initial,
        (stacked[0], stacked[1], stacked[2], jnp.arange(count_blocks, dtype=jnp.int32)),
    )
    maxima, totals, accums = result_state
    map_means = accums / totals[..., None]
    lambda_local = lax.dynamic_slice_in_dim(lambda_head, tp_index * local_heads, local_heads, 0)
    differed = map_means[0] - lambda_local[None, :, None] * map_means[1]
    scaled = (
        differed
        * lax.rsqrt(jnp.mean(differed * differed, axis=-1, keepdims=True) + head_floor)
        * head_gain
        * head_scale
    )
    attn_out = scaled.reshape(tok_rows, local_heads * VALUE_DIM).astype(jnp.bfloat16)
    pool_rows = pool_proj.astype(jnp.bfloat16)
    prior_rows = from_behind(pool_rows[tok_rows - pool_reach :], "sp", 1)
    extended = jnp.concatenate([prior_rows, pool_rows], axis=0).astype(jnp.float32)
    group_ids = tp_index * local_groups + jnp.arange(local_groups, dtype=jnp.int32)
    windows = jnp.left_shift(2, group_ids % 4)
    channel_windows = (windows[:, None] + jnp.zeros((1, GROUP_DIM), jnp.int32)).reshape(-1)
    window_sum = jnp.zeros((tok_rows, local_groups * GROUP_DIM), jnp.float32)
    for lag_steps in range(pool_reach + 1):
        keep_mask = (lag_steps < channel_windows).astype(jnp.float32)
        window_sum = (
            window_sum
            + extended[pool_reach - lag_steps : pool_reach - lag_steps + tok_rows]
            * keep_mask[None, :]
        )
    counts = jnp.minimum(positions[:, None] + 1, channel_windows[None, :]).astype(jnp.float32)
    window_mean = window_sum / counts - pool_rows.astype(jnp.float32)
    local_mixing = lax.dynamic_slice_in_dim(group_weight, tp_index * local_groups, local_groups, 0)
    grouped = jnp.einsum(
        "tgc,gcd->tgd",
        window_mean.astype(jnp.bfloat16).reshape(tok_rows, local_groups, GROUP_DIM),
        local_mixing,
        preferred_element_type=jnp.float32,
    )
    scale_local = lax.dynamic_slice_in_dim(
        pool_scale, tp_index * local_groups * GROUP_DIM, local_groups * GROUP_DIM, 0
    )
    pooled = (grouped.reshape(tok_rows, local_groups * GROUP_DIM) * scale_local).astype(
        jnp.bfloat16
    )
    attn_cols, pool_cols = rows_first((out_attn, out_pool), "sp", (1, 1))
    mixed = sum_at_owner(
        (
            jnp.dot(attn_out, attn_cols, preferred_element_type=jnp.float32)
            + jnp.dot(pooled, pool_cols, preferred_element_type=jnp.float32)
        ).astype(jnp.bfloat16),
        "tp",
        0,
    )
    return mixed.astype(jnp.bfloat16)


def solution(mesh):
    in_specs = (
        P("sp", "tp"),
        P(),
        P("sp", "tp"),
        P("sp", "tp"),
        P("sp", "tp"),
        P("sp", "tp"),
        P("sp", "tp"),
        P("sp", "tp"),
        P(),
        P(),
        P(),
        P(),
        P("tp", "sp"),
        P("tp", "sp"),
    )
    out_specs = P(("sp", "tp"), None)
    return jax.shard_map(body, mesh=mesh, in_specs=in_specs, out_specs=out_specs, check_vma=False)
```

profile of v0, /device:TPU:1, one launch (start us, length us, event | category | flops | bytes accessed | tf_op | source)
XLA Modules:
  0.0 435.4 jit_solution(8674395508657342302)
XLA Ops:
  11.5 2.0 broadcast_in_dim.37
  13.5 5.0 %all-to-all-start = ((bf16[4,256,512]{2,1,0:T(8,128)(2,1)}), bf16[4,256,512]{2,1,0:T(8,128)(2,1)S(1)}, u32[]{:S(2)}, u32[]{:S(2)}) async-start(bf16[4,256,512]{2,1,0:T(8,128)(2,1)} %broadcast_in_dim.37), calls=%async_computation | async-start | bytes 2097152 | tf_op jit(solution)/shard_map/all_to_all | solution.py:30
  19.4 12.6 %all-to-all-done = bf16[4,256,512]{2,1,0:T(8,128)(2,1)S(1)} async-done(((bf16[4,256,512]{2,1,0:T(8,128)(2,1)}), bf16[4,256,512]{2,1,0:T(8,128)(2,1)S(1)}, u32[]{:S(2)}, u32[]{:S(2)}) %all-to-all-start) | async-done | bytes 1048608 | tf_op jit(solution)/shard_map/all_to_all | solution.py:30
  33.6 61.3 %all-gather.4.cloned.1.call-done = bf16[2048,1024]{1,0:T(8,128)(2,1)} async-done(((bf16[32,1024]{1,0:T(8,128)(2,1)}), bf16[2048,1024]{1,0:T(8,128)(2,1)}) %all-gather.4.cloned.1.call-update) | async-done | bytes 4194320 | tf_op jit(solution)/shard_map/all_gather | solution.py:40
  94.8 2.8 slice_bitcast_fusion
  104.3 1.7 convolution_convert_fusion.1
  108.6 1.7 convolution_convert_fusion
  110.3 2.0 collective-permute-start
  114.3 95.5 %all-gather.6.cloned.1.call-done = bf16[16384,512]{0,1:T(8,128)(2,1)} async-done(((bf16[256,512]{0,1:T(8,128)(2,1)}), bf16[16384,512]{0,1:T(8,128)(2,1)}) %all-gather.6.cloned.1.call-update) | async-done | bytes 16777232 | tf_op jit(solution)/shard_map/all_gather | solution.py:40
  209.8 4.1 fusion.104
  213.9 2.8 copy.66
  216.7 4.3 copy.49
  220.9 2.8 copy.65
  223.7 4.3 copy.48
  228.0 7.5 %split.51 = bf16[16384,256]{0,1:T(8,128)(2,1)} slice(bf16[16384,512]{0,1:T(8,128)(2,1)} %all-gather.6.cloned.1.call-done), slice={[0:16384], [256:512]} | slice | bytes 16777216 | tf_op jit(solution)/shard_map/split | solution.py:41
  235.5 15.4 %copy.67 = bf16[32,8,16,1024]{3,2,1,0:T(8,128)(2,1)} copy(bf16[32,8,16,1024]{3,1,2,0:T(8,128)(2,1)} %bitcast.281) | data formatting | bytes 16777216
  250.9 11.6 %copy.50 = bf16[16,1024,2,128]{1,3,2,0:T(8,128)(2,1)} copy(bf16[16,1024,2,128]{1,0,3,2:T(8,128)(2,1)} %bitcast.282) | data formatting | bytes 16777216
  262.5 143.7 %while.15 = (s32[]{:T(128)}, f32[2,256,2]{1,2,0:T(2,128)S(1)}, f32[2,256,2]{1,2,0:T(2,128)S(1)}, f32[2,256,2,128]{1,3,2,0:T(8,128)S(1)}, s32[16]{0:T(128)S(1)}, ...) while((s32[]{:T(128)}, f32[2,256,2]{1,2,0:T(2,128)S(1)}, ...), condition=%wide.region_6.7_spmd.clone, body=%wide.region_1.6_spmd.clone.sunk | while | flops 416947456 | bytes 18045108 | solution.py:182
  267.2 1.9 fusion.147
  269.7 1.7 fusion.150
  276.2 1.9 fusion.147
  278.7 1.7 fusion.150
  285.2 1.9 fusion.147
  287.7 1.7 fusion.150
  294.2 1.9 fusion.147
  296.7 1.7 fusion.150
  303.2 1.9 fusion.147
  305.7 1.7 fusion.150
  312.1 1.9 fusion.147
  314.7 1.7 fusion.150
  321.1 1.9 fusion.147
  330.1 1.9 fusion.147
  332.6 1.7 fusion.150
  339.1 1.9 fusion.147
  341.6 1.7 fusion.150
  348.0 1.9 fusion.147
  350.6 1.7 fusion.150
  357.0 1.9 fusion.147
  359.5 1.7 fusion.150
  366.0 1.9 fusion.147
  368.5 1.7 fusion.150
  375.0 1.9 fusion.147
  377.5 1.7 fusion.150
  383.9 1.9 fusion.147
  392.9 1.9 fusion.147
  401.9 1.9 fusion.147
  406.6 1.9 fusion.49
  409.0 18.5 %all_to_all.10 = bf16[4,64,2048]{2,1,0:T(8,128)(2,1)S(1)} all-to-all(bf16[4,64,2048]{2,1,0:T(8,128)(2,1)S(1)} %bitcast.291), channel_id=1, replica_groups=mesh['sp'=64,'tp'=4] {'tp'}, dimensions={0} | all-to-all | bytes 2097152 | tf_op jit(solution)/shard_map/all_to_all | solution.py:71
  (274 shorter events, 100.7 us)
Async XLA Ops:
  6.5 106.9 %copy-start = (bf16[8,128,128]{2,1,0:T(8,128)(2,1)S(1)}, bf16[8,128,128]{2,1,0:T(8,128)(2,1)}, u32[]{:S(2)}) copy-start(bf16[8,128,128]{2,1,0:T(8,128)(2,1)} %param.26) | copy-start | bytes 786436
  6.5 12.0 %copy-start.5 = (f32[2048]{0:T(1024)S(1)}, f32[2048]{0:T(1024)}, u32[]{:S(2)}) copy-start(f32[2048]{0:T(1024)} %param.17) | copy-start | bytes 24580
  6.5 88.3 %all-gather.4.cloned.1.call-start = ((), (), s32[]{:S(2)}) async-start(), calls=%async_computation.2 | async-start | bytes 4259840 | tf_op jit(solution)/shard_map/all_gather | solution.py:40
  10.8 0.6 copy-start.4
  13.5 18.5 %all-to-all-start = ((bf16[4,256,512]{2,1,0:T(8,128)(2,1)}), bf16[4,256,512]{2,1,0:T(8,128)(2,1)S(1)}, u32[]{:S(2)}, u32[]{:S(2)}) async-start(bf16[4,256,512]{2,1,0:T(8,128)(2,1)} %broadcast_in_dim.37), calls=%async_computation | async-start | bytes 2097152 | tf_op jit(solution)/shard_map/all_to_all | solution.py:30
  18.5 191.3 %all-gather.6.cloned.1.call-start = ((), (), s32[]{:S(2)}) async-start(), calls=%async_computation.3 | async-start | bytes 17039360 | tf_op jit(solution)/shard_map/all_gather | solution.py:40
  100.4 2.3 copy-start.3
  104.2 2.6 copy-start.6
  104.2 2.6 copy-start.7
  104.3 3.5 copy-start.9
  104.3 4.3 copy-start.8
  106.8 299.8 %all-gather.8.cloned.1.call-start = ((), (), s32[]{:S(2)}) async-start(), calls=%async_computation.4 | async-start | bytes 2129920 | tf_op jit(solution)/shard_map/all_gather | solution.py:54
  110.3 3.1 collective-permute-start
  406.6 1.9 copy-start.2
  408.5 19.9 %copy-start.1 = (bf16[8,128,128]{2,1,0:T(8,128)(2,1)S(1)}, bf16[8,128,128]{2,1,0:T(8,128)(2,1)}, u32[]{:S(2)}) copy-start(bf16[8,128,128]{2,1,0:T(8,128)(2,1)} %param.26) | copy-start | bytes 786436
Sparse Core Ops, SparseCore 0:
  11.6 83.1 all-gather.3
  106.9 102.8 all-gather.5
  212.6 75.7 all-gather.7
where the time goes:
time: 444 us; the launch traced here: 435 us
  waiting for transfers between devices  171 us (39%)
  matrix products  118 us (27%)
  local copies, waits for them, and re-layouts  76.4 us (17%)
  other arithmetic  19.5 us (4%)
  blocking collectives  18.5 us (4%)
  between operations  13.9 us (3%)
  loops' own time  12 us (3%)
  starting transfers between devices  7.04 us (2%)
    all_gather x2, waiting for transfers between devices, side_by_side(): out = lax.all_gather(both, axis, axis=dim, tiled=True)  157 us
    dot_general x32, matrix products, step_block(): jnp.einsum('qhd,khd->qhk', queries[map_index], key_part, preferred_elemen...  54.5 us
    dot_general x32, matrix products, step_block(): jnp.einsum('qhk,khd->qhd', weights.astype(jnp.bfloat16), block_v, preferr...  54 us
    unnamed x31, local copies, waits for them, and re-layouts  45.3 us
    all_to_all x1, blocking collectives, sum_at_owner(): blocks = lax.all_to_all(in_blocks(x, dim, peers), axis, 0, 0, tiled=True)  18.5 us
    all_to_all x1, waiting for transfers between devices, from_everyone(): lax.all_to_all(jnp.broadcast_to(x[None], (peers, *x.shape)), axis, 0, 0,...  12.6 us
    another operation x1, loops' own time, body(): lax.scan(step_block, initial, (stacked[0], stacked[1], stacked[2], jnp.ar...  12 us
    split x2, local copies, waits for them, and re-layouts, side_by_side(): jnp.split(out, [sum(widths[:k]) for k in range(1, len(widths))], axis=along)  11.6 us
  transfers between devices with their start and end apart: 5, of which 4 were waited for; matrix products, arithmetic and copies ran while one was open for 44% of the time, Pallas kernels for 0%

commit v1 on v0

v1 whole, which is shorter than its diff:
```python
import math

import jax
import jax.numpy as jnp
import numpy as np
from jax import lax
from jax.experimental import pallas as pl
from jax.experimental.pallas import tpu as pltpu
from jax.sharding import PartitionSpec as P

MESH = pl.DeviceIdType.MESH
F32 = jnp.float32
BF16 = jnp.bfloat16
Z_SIZE = 8
X_SIZE = 4
LANE_TILE = 256

rope_base = 500000.0
head_scale = 0.8
norm_floor = 1e-06
head_floor = 0.001
low_score = -1e30


def rope_tables(chip_tokens, chips):
    lane = np.arange(128)
    inverse = rope_base ** (-((lane % 32) * 2.0 / 64.0))
    sign = np.where(lane % 64 < 32, -1.0, 1.0)
    near = np.arange(chip_tokens)[:, None] * inverse[None, :]
    far = (np.arange(chips) * chip_tokens)[:, None] * inverse[None, :]
    return (
        np.cos(near).astype(np.float32),
        (np.sin(near) * sign).astype(np.float32),
        np.cos(far).astype(np.float32),
        (np.sin(far) * sign).astype(np.float32),
    )


class Ring:
    def __init__(self, n, me, device, unit, sems):
        self.n, self.me, self.device, self.unit = n, me, device, unit
        self.sems = {}
        for h in range(1, n // 2 + 1):
            for d in (0, 1):
                for u in (0, 1):
                    if self.has(d, h, u):
                        self.sems[d, h, u] = sems()

    def has(self, d, h, u):
        return h < self.n // 2 or (h == self.n // 2 and d == u)

    def slot(self, d, h):
        sign = 1 if d == 0 else -1
        return lax.rem(self.me - sign * h + self.n, self.n)

    def copy(self, d, h, u, slot):
        ref = self.unit(u, slot)
        send_sem, recv_sem = self.sems[d, h, u]
        return pltpu.make_async_remote_copy(
            src_ref=ref,
            dst_ref=ref,
            send_sem=send_sem,
            recv_sem=recv_sem,
            device_id=self.device(1 if d == 0 else -1),
            device_id_type=MESH,
        )

    def send(self, d, h, u):
        self.copy(d, h, u, self.slot(d, h - 1)).start()

    def begin(self, units=(0, 1)):
        for u in units:
            for d in (0, 1):
                if self.has(d, 1, u):
                    self.send(d, 1, u)

    def step(self, h):
        for u in (0, 1):
            for d in (0, 1):
                if self.has(d, h, u):
                    self.copy(d, h, u, self.slot(d, h)).wait_recv()
                    if (d, h + 1, u) in self.sems:
                        self.send(d, h + 1, u)

    def finish(self):
        for d, h, u in self.sems:
            self.copy(d, h, u, self.slot(d, h - 1)).wait_send()


def dot(a, b, dims=((1,), (0,))):
    return lax.dot_general(a, b, (dims, ((), ())), preferred_element_type=F32)


def make_kernel(zs, xs, ys, tok, wide):
    chip = 2 * tok
    kz = wide // zs
    part = wide // ys
    kb = min(kz, part)
    quarter = tok // ys
    tiles = 2 * chip // LANE_TILE

    def kernel(
        tokens, gain, q1, k1, q2, k2, vw, pw, lam, hgain, gw, pscale, oa, op,
        cos_near, sin_near, cos_far, sin_far,
        out,
        wsend, wbuf, wt, tokbuf, nrm, proj, kbuf, vbuf, qz, acc, mbuf, lbuf,
        pext, halo_x, halo_z, o1s, e1s, o1r, e1r, o2s, e2s, o2r, e2r, abuf,
        ysum, y1r, y2s, y2r, send_sems, recv_sems,
    ):
        sp = lax.axis_index("sp")
        y = lax.axis_index("tp")
        core = lax.rem(sp, 2)
        place = sp // 2
        x = lax.rem(place, xs)
        z = place // xs
        other = 1 - core
        head = 2 * y + core

        def at_z(step):
            return {"sp": (lax.rem(z + step + zs, zs) * xs + x) * 2 + core, "tp": y}

        def at_x(step):
            return {"sp": (z * xs + lax.rem(x + step + xs, xs)) * 2 + core, "tp": y}

        def at_y(step):
            return {"sp": sp, "tp": lax.rem(y + step + ys, ys)}

        def at_partner():
            return {"sp": place * 2 + other, "tp": y}

        used = [0]

        def sems():
            k = used[0]
            used[0] += 1
            return send_sems.at[k], recv_sems.at[k]

        def remote(src, dst, device):
            send_sem, recv_sem = sems()
            return pltpu.make_async_remote_copy(
                src_ref=src, dst_ref=dst, send_sem=send_sem, recv_sem=recv_sem,
                device_id=device, device_id_type=MESH,
            )

        sent = []

        def post(copy):
            copy.start()
            sent.append(copy)
            return copy

        def by_head(h):
            a, b = h * 64, h * 64 + 64
            c, d = h * 128, h * 128 + 128
            return jnp.concatenate(
                [q1[:, a:b], q2[:, a:b], k1[:, a:b], k2[:, a:b], vw[:, c:d], pw[:, c:d]], axis=1
            )

        rows = q1.shape[0]
        first, second = by_head(0), by_head(1)
        mine = core == 0
        wbuf[z, x, pl.ds(core * rows, rows), :] = jnp.where(mine, first, second)
        wsend[...] = jnp.where(mine, second, first)
        tokbuf[core, y] = tokens[...]
        qz[...] = jnp.zeros_like(qz)
        mbuf[...] = jnp.full(mbuf.shape, low_score, F32)
        lbuf[...] = jnp.zeros_like(lbuf)
        acc[...] = jnp.zeros_like(acc)

        barrier = pltpu.get_barrier_semaphore()
        neighbours = [at_z(1), at_z(-1), at_x(1), at_x(-1), at_y(1), at_y(-1), at_partner()]
        for device in neighbours:
            pl.semaphore_signal(barrier, inc=1, device_id=device, device_id_type=MESH)
        pl.semaphore_wait(barrier, len(neighbours))

        w_swap = post(
            remote(wsend, wbuf.at[z, x, pl.ds(core * rows, rows), :], at_partner())
        )
        half = tok // 2
        tok_ring = Ring(
            ys, y, at_y, lambda u, s: tokbuf.at[core, s, pl.ds(u * half, half), :], sems
        )
        tok_ring.begin()

        def share_tokens(s):
            return post(remote(tokbuf.at[core, s], tokbuf.at[core, s], at_partner()))

        shared = [share_tokens(y)]

        w_ring_x = Ring(
            xs, x, at_x, lambda u, s: wbuf.at[z, s, pl.ds(u * rows, rows), :], sems
        )
        w_ring_z = Ring(
            zs, z, at_z, lambda u, s: wbuf.at[s, pl.ds(u * (xs // 2), xs // 2)], sems
        )
        w_swap.wait_recv()
        w_ring_x.begin()

        eye = (
            lax.broadcasted_iota(jnp.int32, (rows, rows), 0)
            == lax.broadcasted_iota(jnp.int32, (rows, rows), 1)
        ).astype(BF16)
        oat = dot(eye, oa[...], ((1,), (1,))).astype(BF16)
        opt = dot(eye, op[...], ((1,), (1,))).astype(BF16)
        wt[z, x, core] = jnp.concatenate(
            [oat[:, :128], opt[:, :128], oat[:, 128:], opt[:, 128:]], axis=1
        )
        cb, sb = cos_far[pl.ds(place, 1), :], sin_far[pl.ds(place, 1), :]

        for h in range(1, xs // 2 + 1):
            w_ring_x.step(h)
        w_ring_z.begin()

        wt_half = rows // 2
        wt_ring_z = Ring(
            zs, z, at_z, lambda u, s: wt.at[s, x, core, pl.ds(u * wt_half, wt_half), :], sems
        )
        wt_ring_x = Ring(
            xs, x, at_x, lambda u, s: wt.at[pl.ds(u * (zs // 2), zs // 2), s, core], sems
        )

        for h in range(1, ys // 2 + 1):
            tok_ring.step(h)
            if h < ys // 2:
                shared.append(share_tokens(tok_ring.slot(0, h)))
                shared.append(share_tokens(tok_ring.slot(1, h)))
            else:
                shared.append(share_tokens(tok_ring.slot(0, h)))
        for copy in shared:
            copy.wait_recv()

        per_part = part // kb
        for owner in range(2):
            square = jnp.zeros((tok, 1), F32)
            for s in range(ys):
                block = tokbuf[owner, s].astype(F32)
                square = square + jnp.sum(block * block, axis=1, keepdims=True)
            scale = lax.rsqrt(square * (1.0 / wide) + norm_floor)
            for s in range(ys):
                block = tokbuf[owner, s].astype(F32) * scale * gain[:, s * part : (s + 1) * part]
                for j in range(per_part):
                    nrm[s * per_part + j, owner * tok : (owner + 1) * tok, :] = block[
                        :, j * kb : (j + 1) * kb
                    ].astype(BF16)

        def project(s, start):
            weight = wbuf[s].reshape(kz, 512)
            per_slot = kz // kb
            term = dot(nrm[s * per_slot], weight[0:kb])
            for j in range(1, per_slot):
                term = term + dot(nrm[s * per_slot + j], weight[j * kb : (j + 1) * kb])
            if start:
                proj[...] = term
            else:
                proj[...] += term

        project(z, True)
        for h in range(1, zs // 2 + 1):
            w_ring_z.step(h)
            project(w_ring_z.slot(0, h), False)
            if h < zs // 2:
                project(w_ring_z.slot(1, h), False)

        ca, sa = cos_near[...], sin_near[...]
        cosine = ca * cb - sa * sb
        sine = sa * cb + ca * sb
        low = lax.rem(lax.broadcasted_iota(jnp.int32, (chip, 128), 1), 64) < 32

        def turned(v):
            swapped = jnp.where(low, pltpu.roll(v, 96, 1), pltpu.roll(v, 32, 1))
            return v * cosine + swapped * sine

        kbuf[z] = turned(proj[:, 128:256]).astype(BF16)
        vbuf[z] = proj[:, 256:384].T.astype(BF16)
        kv_ring = Ring(
            zs, z, at_z, lambda u, s: (kbuf.at[s] if u == 0 else vbuf.at[s]), sems
        )
        kv_ring.begin()
        queries = (turned(proj[:, 0:128]) * (0.125 * math.log2(math.e))).T.astype(BF16)
        qz[x, 0:64, 0:chip] = queries[0:64]
        qz[x, 64:128, chip : 2 * chip] = queries[64:128]
        q_ring = Ring(
            xs, x, at_x,
            lambda u, s: qz.at[s, pl.ds(64 * u, 64), pl.ds(chip * u, chip)], sems,
        )
        q_ring.begin()

        pool = proj[:, 384:512].astype(BF16)
        pext[16 : 16 + chip, :] = pool.astype(F32)
        halo_x[0] = pool[chip - 16 :, :]
        to_x = post(remote(halo_x.at[0], halo_x.at[1], at_x(1)))
        wt_ring_z.begin()

        def tile(slot, ch, lt, masked):
            lanes = pl.ds(lt * LANE_TILE, LANE_TILE)
            s = dot(kbuf[slot], qz[ch, :, lanes])
            if masked:
                offset = (lt * LANE_TILE) % chip
                visible = lax.broadcasted_iota(jnp.int32, s.shape, 0) <= (
                    lax.broadcasted_iota(jnp.int32, s.shape, 1) + offset
                )
                s = jnp.where(visible, s, low_score)
            before = mbuf[ch, 0:1, lanes]
            now = jnp.maximum(before, jnp.max(s, axis=0, keepdims=True))
            p = jnp.exp2(s - now)
            factor = jnp.exp2(before - now)
            mbuf[ch, 0:1, lanes] = now
            lbuf[ch, 0:1, lanes] = lbuf[ch, 0:1, lanes] * factor + jnp.sum(
                p, axis=0, keepdims=True
            )
            acc[ch, :, lanes] = acc[ch, :, lanes] * factor + dot(vbuf[slot], p.astype(BF16))

        def attend(slot, start):
            def chunk(ch, carry):
                for lt in range(tiles):
                    tile(slot, ch, lt, False)
                return carry

            lax.fori_loop(start, xs, chunk, 0)

        for lt in range(tiles):
            tile(z, x, lt, True)

        to_x.wait_recv()
        to_z = post(remote(halo_x.at[1], halo_z, at_z(1)))
        for h in range(1, xs // 2 + 1):
            q_ring.step(h)
        to_z.wait_recv()
        from_x, from_z = halo_x[1].astype(F32), halo_z[...].astype(F32)
        prior = jnp.where(x == 0, from_z, from_x)
        pext[0:16, :] = jnp.where(place == 0, 0.0, prior)
        window = jnp.left_shift(2, lax.rem(head, 4))
        whole = pext[...]
        run = whole
        window_sum = jnp.zeros((chip, 128), F32)
        for k in range(4):
            lag = 1 << k
            run = run + jnp.concatenate(
                [jnp.zeros((lag, 128), F32), run[: 16 + chip - lag]], axis=0
            )
            window_sum = jnp.where(window == 2 * lag, run[16:], window_sum)
        position = place * chip + lax.broadcasted_iota(jnp.int32, (chip, 128), 0)
        count = jnp.minimum(position + 1, window).astype(F32)
        window_mean = (window_sum / count - whole[16:]).astype(BF16)
        pooled = (dot(window_mean, gw[head]) * pscale[pl.ds(head, 1), :]).astype(BF16)
        abuf[0, :, 128:256] = pooled[0:tok]
        abuf[1, :, 128:256] = pooled[tok:]
        attend(z, x + 1)

        for h in range(1, zs // 2 + 1):
            kv_ring.step(h)
            wt_ring_z.step(h)
            if h == zs // 2:
                wt_ring_x.begin()
            up, down = kv_ring.slot(0, h), kv_ring.slot(1, h)

            @pl.when(up < z)
            def _():
                attend(up, 0)

            if h < zs // 2:

                @pl.when(down < z)
                def _():
                    attend(down, 0)

        wt_shared = [
            post(remote(wt.at[:, x, core], wt.at[:, x, core], at_partner()))
        ]
        for h in range(1, xs // 2 + 1):
            wt_ring_x.step(h)
            for d in (0, 1):
                if h < xs // 2 or d == 0:
                    s = wt_ring_x.slot(d, h)
                    wt_shared.append(
                        post(remote(wt.at[:, s, core], wt.at[:, s, core], at_partner()))
                    )

        def share(ch, m):
            lanes = pl.ds(m * chip, chip)
            total = lbuf[ch, 0:1, lanes]
            some = total > 0.0
            safe = jnp.where(some, total, 1.0)
            weight = jnp.where(some, mbuf[ch, 0:1, lanes] + jnp.log2(safe), low_score)
            return acc[ch, :, lanes] * (1.0 / safe), weight

        def joined(*shares):
            top = shares[0][1]
            for _, weight in shares[1:]:
                top = jnp.maximum(top, weight)
            factors = [jnp.exp2(weight - top) for _, weight in shares]
            total = sum(factors)
            value = sum(o * f for (o, _), f in zip(shares, factors)) * (1.0 / total)
            return value, top + jnp.log2(total)

        def put(pair, o_ref, e_ref):
            o_ref[...] = pair[0].astype(BF16)
            e_ref[...] = jnp.broadcast_to(pair[1], e_ref.shape)

        def send_pair(o_src, e_src, o_dst, e_dst, device):
            return post(remote(o_src, o_dst, device)), post(remote(e_src, e_dst, device))

        def get(o_ref, e_ref):
            return o_ref[...].astype(F32), e_ref[0:1, :]

        ahead = lax.rem(x + 1, xs)
        behind = lax.rem(x + xs - 1, xs)
        across = lax.rem(x + 2, xs)
        sides = ((ahead, at_x(1)), (behind, at_x(-1)))
        first_hop = []
        for m in (0, 1):
            put(share(across, m), o1s.at[m], e1s.at[m])
            first_hop.append(
                send_pair(o1s.at[m], e1s.at[m], o1r.at[m], e1r.at[m], sides[m][1])
            )
        second_hop = []
        for m in (0, 1):
            chunk, device = sides[m]
            k = 1 - m
            put(share(chunk, k), o2s.at[m, k], e2s.at[m, k])
            second_hop.append(
                send_pair(o2s.at[m, k], e2s.at[m, k], o2r.at[m, k], e2r.at[m, k], device)
            )
        for m in (0, 1):
            for copy in first_hop[m]:
                copy.wait_recv()
            chunk, device = sides[m]
            put(joined(share(chunk, m), get(o1r.at[m], e1r.at[m])), o2s.at[m, m], e2s.at[m, m])
            second_hop.append(
                send_pair(o2s.at[m, m], e2s.at[m, m], o2r.at[m, m], e2r.at[m, m], device)
            )
        for pair in second_hop:
            for copy in pair:
                copy.wait_recv()
        means = [
            joined(
                share(x, m),
                get(o2r.at[0, m], e2r.at[0, m]),
                get(o2r.at[1, m], e2r.at[1, m]),
            )[0]
            for m in (0, 1)
        ]
        difference = means[0] - lam[head] * means[1]
        norm = lax.rsqrt(jnp.mean(difference * difference, axis=0, keepdims=True) + head_floor)
        attn = ((difference * norm).T * hgain[...] * head_scale).astype(BF16)

        abuf[0, :, 0:128] = attn[0:tok]
        abuf[1, :, 0:128] = attn[tok:]
        swap = post(remote(abuf.at[other], abuf.at[2], at_partner()))
        swap.wait_recv()
        for copy in wt_shared:
            copy.wait_recv()

        own_rows = abuf[core]
        their_rows = abuf[2]
        rows_0 = jnp.where(core == 0, own_rows, their_rows)
        rows_1 = jnp.where(core == 0, their_rows, own_rows)
        per_z = wide // zs
        for s in range(zs):
            weight = wt[s].reshape(per_z, 512)
            ysum[:, s * per_z : (s + 1) * per_z] = (
                dot(rows_0, weight[:, 0:256], ((1,), (1,)))
                + dot(rows_1, weight[:, 256:512], ((1,), (1,)))
            ).astype(BF16)

        y_half = quarter // 2
        y_across = lax.rem(y + 2, ys)
        y_sides = (
            (lax.rem(y + 1, ys), at_y(1)),
            (lax.rem(y + ys - 1, ys), at_y(-1)),
        )

        def rows_of(target, m):
            return pl.ds(target * quarter + m * y_half, y_half)

        y_first, y_second = [], []
        for m in (0, 1):
            y_first.append(
                post(remote(ysum.at[rows_of(y_across, m), :], y1r.at[m], y_sides[m][1]))
            )
        for m in (0, 1):
            target, device = y_sides[m]
            y_second.append(
                post(remote(ysum.at[rows_of(target, 1 - m), :], y2r.at[m, 1 - m], device))
            )
        for m in (0, 1):
            target, device = y_sides[m]
            y_first[m].wait_recv()
            y2s[m] = (
                ysum[rows_of(target, m), :].astype(F32) + y1r[m].astype(F32)
            ).astype(BF16)
            y_second.append(post(remote(y2s.at[m], y2r.at[m, m], device)))
        for copy in y_second:
            copy.wait_recv()
        for m in (0, 1):
            out[m * y_half : (m + 1) * y_half, :] = (
                ysum[rows_of(y, m), :].astype(F32)
                + y2r[0, m].astype(F32)
                + y2r[1, m].astype(F32)
            ).astype(BF16)

        for copy in sent:
            copy.wait_send()
        for ring in (tok_ring, w_ring_x, w_ring_z, wt_ring_x, wt_ring_z, kv_ring, q_ring):
            ring.finish()

    return kernel


def solution(mesh):
    sp_size, ys = mesh.shape["sp"], mesh.shape["tp"]
    zs, xs = Z_SIZE, X_SIZE
    assert zs * xs * 2 == sp_size

    def body(
        tokens, norm_gain, query_one, key_one, query_two, key_two, value_weight, pool_weight,
        lambda_head, head_gain, group_weight, pool_scale, out_attn, out_pool,
    ):
        tok, part = tokens.shape
        wide = part * ys
        chip = 2 * tok
        rows = query_one.shape[0]
        quarter = tok // ys
        tables = rope_tables(chip, zs * xs)
        vmem = pl.BlockSpec(memory_space=pltpu.VMEM)
        smem = pl.BlockSpec(memory_space=pltpu.SMEM)
        args = (
            tokens, norm_gain.reshape(1, wide), query_one, key_one, query_two, key_two,
            value_weight, pool_weight, lambda_head, head_gain.reshape(1, 128), group_weight,
            pool_scale.reshape(-1, 128), out_attn, out_pool, *tables,
        )
        specs = [vmem] * len(args)
        specs[8] = smem
        semaphores = 128
        return pl.pallas_call(
            make_kernel(zs, xs, ys, tok, wide),
            out_shape=jax.ShapeDtypeStruct((quarter, wide), BF16),
            in_specs=specs,
            out_specs=vmem,
            scratch_shapes=[
                pltpu.VMEM((rows, 512), BF16),
                pltpu.VMEM((zs, xs, 2 * rows, 512), BF16),
                pltpu.VMEM((zs, xs, 2, rows, 512), BF16),
                pltpu.VMEM((2, ys, tok, part), BF16),
                pltpu.VMEM((max(zs, ys), chip, wide // max(zs, ys)), BF16),
                pltpu.VMEM((chip, 512), F32),
                pltpu.VMEM((zs, chip, 128), BF16),
                pltpu.VMEM((zs, 128, chip), BF16),
                pltpu.VMEM((xs, 128, 2 * chip), BF16),
                pltpu.VMEM((xs, 128, 2 * chip), F32),
                pltpu.VMEM((xs, 8, 2 * chip), F32),
                pltpu.VMEM((xs, 8, 2 * chip), F32),
                pltpu.VMEM((16 + chip, 128), F32),
                pltpu.VMEM((2, 16, 128), BF16),
                pltpu.VMEM((16, 128), BF16),
                pltpu.VMEM((2, 128, chip), BF16),
                pltpu.VMEM((2, 8, chip), F32),
                pltpu.VMEM((2, 128, chip), BF16),
                pltpu.VMEM((2, 8, chip), F32),
                pltpu.VMEM((2, 2, 128, chip), BF16),
                pltpu.VMEM((2, 2, 8, chip), F32),
                pltpu.VMEM((2, 2, 128, chip), BF16),
                pltpu.VMEM((2, 2, 8, chip), F32),
                pltpu.VMEM((3, tok, 256), BF16),
                pltpu.VMEM((tok, wide), BF16),
                pltpu.VMEM((2, quarter // 2, wide), BF16),
                pltpu.VMEM((2, quarter // 2, wide), BF16),
                pltpu.VMEM((2, 2, quarter // 2, wide), BF16),
                pltpu.SemaphoreType.DMA((semaphores,)),
                pltpu.SemaphoreType.DMA((semaphores,)),
            ],
            compiler_params=pltpu.CompilerParams(
                collective_id=0, has_side_effects=True, vmem_limit_bytes=60 * 1024 * 1024
            ),
            name="mixer",
        )(*args)

    in_specs = (
        P("sp", "tp"),
        P(),
        P("sp", "tp"),
        P("sp", "tp"),
        P("sp", "tp"),
        P("sp", "tp"),
        P("sp", "tp"),
        P("sp", "tp"),
        P(),
        P(),
        P(),
        P(),
        P("tp", "sp"),
        P("tp", "sp"),
    )
    out_specs = P(("sp", "tp"), None)
    return jax.shard_map(body, mesh=mesh, in_specs=in_specs, out_specs=out_specs, check_vma=False)
```

time: 444 us -> 135 us (0.30)
  the two profiles are of different devices: /device:TPU:1 before, /device:TPU:225 now
where the time goes in v1:
time: 135 us
  Pallas kernels  131 us (97%)
  local copies, waits for them, and re-layouts  3.86 us (3%)
    pallas_call x1, Pallas kernels, body(): pl.pallas_call(make_kernel(zs, xs, ys, tok, wide), out_shape=jax.ShapeDty...  131 us
    unnamed x5, local copies, waits for them, and re-layouts  3.86 us

profile of v1, /device:TPU:225, one launch (start us, length us, event | category | flops | bytes accessed | tf_op | source)
XLA Modules:
  0.0 134.9 jit_solution(7984791579553038117)
XLA Ops:
  0.0 0.0 copy-start
  0.0 1.5 %copy.19.oa = bf16[256,32]{1,0:T(8,128)(2,1)} copy(bf16[256,32]{0,1:T(8,128)(2,1)} %param.30) | data formatting | bytes 32768 | tf_op args[12]
  1.5 0.0 copy-done
  1.5 0.7 copy.20.op
  2.2 131.1 %mixer.1 = bf16[64,2048]{1,0:T(8,128)(2,1)} custom-call(bf16[256,512]{1,0:T(8,128)(2,1)} %tokens.1, f32[1,2048]{1,0:T(1,128)} %bitcast.3, bf16[32,128]{1,0:T(8,128)(2,1)} %q1.1, bf16[32,128]{1,0:T(8,128)(2,1)} %k1.1, bf16[32,128]{1,0:T(8,128)(2,1)} %q2.1, bf16[32,128]{1,0:T(8,128)(2,1)} %k2.1, bf16[32,256]{1,0:T(8,128)(2,1)} %vw.1, bf16[32,256]{1,0:T(8,128)(2,1)} %pw.1, ...), custom_call_target="tpu_custom_call" | custom-call | tf_op jit(solution)/shard_map/mixer/pallas_call | solution.py:535
  133.3 1.7 %copy.22 = bf16[64,2048]{1,0:T(8,128)(2,1)} copy(bf16[64,2048]{1,0:T(8,128)(2,1)} %mixer.1) | data formatting | bytes 524288
Async XLA Ops:
  0.0 1.5 %copy-start = (bf16[256,32]{0,1:T(8,128)(2,1)S(1)}, bf16[256,32]{0,1:T(8,128)(2,1)}, u32[]{:S(2)}) copy-start(bf16[256,32]{0,1:T(8,128)(2,1)} %param.31) | copy-start | bytes 49156

commit v2 on v1

--- a/solution.py
+++ b/solution.py
@@ -93,9 +93,7 @@
 
 def make_kernel(zs, xs, ys, tok, wide):
     chip = 2 * tok
-    kz = wide // zs
     part = wide // ys
-    kb = min(kz, part)
     quarter = tok // ys
     tiles = 2 * chip // LANE_TILE
 
@@ -104,7 +102,7 @@
         cos_near, sin_near, cos_far, sin_far,
         out,
         wsend, wbuf, wt, tokbuf, nrm, proj, kbuf, vbuf, qz, acc, mbuf, lbuf,
-        pext, halo_x, halo_z, o1s, e1s, o1r, e1r, o2s, e2s, o2r, e2r, abuf,
+        pext, halo, o1s, e1s, o1r, e1r, o2s, e2s, o2r, e2r, abuf,
         ysum, y1r, y2s, y2r, send_sems, recv_sems,
     ):
         sp = lax.axis_index("sp")
@@ -125,6 +123,10 @@
         def at_y(step):
             return {"sp": sp, "tp": lax.rem(y + step + ys, ys)}
 
+        def at_chip(step):
+            chips = zs * xs
+            return {"sp": lax.rem(place + step + chips, chips) * 2 + core, "tp": y}
+
         def at_partner():
             return {"sp": place * 2 + other, "tp": y}
 
@@ -159,77 +161,104 @@
         rows = q1.shape[0]
         first, second = by_head(0), by_head(1)
         mine = core == 0
-        wbuf[z, x, pl.ds(core * rows, rows), :] = jnp.where(mine, first, second)
+        own_rows = pl.ds(core * rows, rows)
+        their_rows = pl.ds(other * rows, rows)
+        wbuf[z, x, own_rows, :] = jnp.where(mine, first, second)
         wsend[...] = jnp.where(mine, second, first)
         tokbuf[core, y] = tokens[...]
+        wt[z, x, core] = jnp.concatenate(
+            [oa[:, :128], op[:, :128], oa[:, 128:], op[:, 128:]], axis=1
+        )
         qz[...] = jnp.zeros_like(qz)
         mbuf[...] = jnp.full(mbuf.shape, low_score, F32)
         lbuf[...] = jnp.zeros_like(lbuf)
         acc[...] = jnp.zeros_like(acc)
 
         barrier = pltpu.get_barrier_semaphore()
-        neighbours = [at_z(1), at_z(-1), at_x(1), at_x(-1), at_y(1), at_y(-1), at_partner()]
+        neighbours = [
+            at_z(1), at_z(-1), at_x(1), at_x(-1), at_y(1), at_y(-1), at_partner(), at_chip(1), at_chip(-1),
+        ]
         for device in neighbours:
             pl.semaphore_signal(barrier, inc=1, device_id=device, device_id_type=MESH)
         pl.semaphore_wait(barrier, len(neighbours))
 
-        w_swap = post(
-            remote(wsend, wbuf.at[z, x, pl.ds(core * rows, rows), :], at_partner())
-        )
+        w_swap = post(remote(wsend, wbuf.at[z, x, own_rows, :], at_partner()))
         half = tok // 2
+        strip = rows // 2
         tok_ring = Ring(
             ys, y, at_y, lambda u, s: tokbuf.at[core, s, pl.ds(u * half, half), :], sems
         )
+        own_x = Ring(
+            xs, x, at_x,
+            lambda u, s: wbuf.at[z, s, pl.ds(core * rows + u * strip, strip), :], sems,
+        )
+        own_z = Ring(
+            zs, z, at_z,
+            lambda u, s: wbuf.at[s, pl.ds(u * (xs // 2), xs // 2), own_rows, :], sems,
+        )
+        their_z = Ring(
+            zs, z, at_z,
+            lambda u, s: wbuf.at[s, x, pl.ds(other * rows + u * strip, strip), :], sems,
+        )
+        wt_ring_z = Ring(
+            zs, z, at_z, lambda u, s: wt.at[s, x, core, pl.ds(u * strip, strip), :], sems
+        )
+        wt_ring_x = Ring(
+            xs, x, at_x, lambda u, s: wt.at[pl.ds(u * (zs // 2), zs // 2), s, core], sems
+        )
+
+        def their_x_ring(slot):
+            ring = Ring(
+                xs, x, at_x,
+                lambda u, s: wbuf.at[slot, s, pl.ds(other * rows + u * strip, strip), :], sems,
+            )
+            ring.begin()
+            return ring
+
+        own_x.begin()
         tok_ring.begin()
 
         def share_tokens(s):
             return post(remote(tokbuf.at[core, s], tokbuf.at[core, s], at_partner()))
 
         shared = [share_tokens(y)]
-
-        w_ring_x = Ring(
-            xs, x, at_x, lambda u, s: wbuf.at[z, s, pl.ds(u * rows, rows), :], sems
-        )
-        w_ring_z = Ring(
-            zs, z, at_z, lambda u, s: wbuf.at[s, pl.ds(u * (xs // 2), xs // 2)], sems
-        )
+        cb, sb = cos_far[pl.ds(place, 1), :], sin_far[pl.ds(place, 1), :]
         w_swap.wait_recv()
-        w_ring_x.begin()
-
-        eye = (
-            lax.broadcasted_iota(jnp.int32, (rows, rows), 0)
-            == lax.broadcasted_iota(jnp.int32, (rows, rows), 1)
-        ).astype(BF16)
-        oat = dot(eye, oa[...], ((1,), (1,))).astype(BF16)
-        opt = dot(eye, op[...], ((1,), (1,))).astype(BF16)
-        wt[z, x, core] = jnp.concatenate(
-            [oat[:, :128], opt[:, :128], oat[:, 128:], opt[:, 128:]], axis=1
-        )
-        cb, sb = cos_far[pl.ds(place, 1), :], sin_far[pl.ds(place, 1), :]
-
-        for h in range(1, xs // 2 + 1):
-            w_ring_x.step(h)
-        w_ring_z.begin()
-
-        wt_half = rows // 2
-        wt_ring_z = Ring(
-            zs, z, at_z, lambda u, s: wt.at[s, x, core, pl.ds(u * wt_half, wt_half), :], sems
-        )
-        wt_ring_x = Ring(
-            xs, x, at_x, lambda u, s: wt.at[pl.ds(u * (zs // 2), zs // 2), s, core], sems
-        )
-
-        for h in range(1, ys // 2 + 1):
+        their_z.begin()
+        their_x = [their_x_ring(z)]
+
+        def their_step(h):
+            their_z.step(h)
+            their_x.append(their_x_ring(their_z.slot(0, h)))
+            if h < zs // 2:
+                their_x.append(their_x_ring(their_z.slot(1, h)))
+
+        def tok_step(h):
             tok_ring.step(h)
+            shared.append(share_tokens(tok_ring.slot(0, h)))
             if h < ys // 2:
-                shared.append(share_tokens(tok_ring.slot(0, h)))
                 shared.append(share_tokens(tok_ring.slot(1, h)))
-            else:
-                shared.append(share_tokens(tok_ring.slot(0, h)))
+
+        own_x.step(1)
+        their_step(1)
+        own_x.step(2)
+        own_z.begin()
+        if zs > 2:
+            their_step(2)
+            their_step(3)
+        tok_step(1)
+        for ring in their_x[:3]:
+            ring.step(1)
+        if zs > 2:
+            their_step(4)
+        own_z.step(1)
+        wt_ring_z.begin()
+        for ring in their_x[:3]:
+            ring.step(2)
+        tok_step(2)
         for copy in shared:
             copy.wait_recv()
 
-        per_part = part // kb
         for owner in range(2):
             square = jnp.zeros((tok, 1), F32)
             for s in range(ys):
@@ -238,29 +267,27 @@
             scale = lax.rsqrt(square * (1.0 / wide) + norm_floor)
             for s in range(ys):
                 block = tokbuf[owner, s].astype(F32) * scale * gain[:, s * part : (s + 1) * part]
-                for j in range(per_part):
-                    nrm[s * per_part + j, owner * tok : (owner + 1) * tok, :] = block[
-                        :, j * kb : (j + 1) * kb
-                    ].astype(BF16)
-
-        def project(s, start):
-            weight = wbuf[s].reshape(kz, 512)
-            per_slot = kz // kb
-            term = dot(nrm[s * per_slot], weight[0:kb])
-            for j in range(1, per_slot):
-                term = term + dot(nrm[s * per_slot + j], weight[j * kb : (j + 1) * kb])
-            if start:
-                proj[...] = term
-            else:
-                proj[...] += term
-
-        project(z, True)
-        for h in range(1, zs // 2 + 1):
-            w_ring_z.step(h)
-            project(w_ring_z.slot(0, h), False)
-            if h < zs // 2:
-                project(w_ring_z.slot(1, h), False)
-
+                nrm[owner * tok : (owner + 1) * tok, s * part : (s + 1) * part] = block.astype(BF16)
+
+        wt_hops = list(range(1, zs // 2 + 1))
+
+        def wt_next():
+            if wt_hops:
+                wt_ring_z.step(wt_hops.pop(0))
+
+        if zs > 2:
+            own_z.step(2)
+            for ring in their_x[3:]:
+                ring.step(1)
+            wt_next()
+            own_z.step(3)
+            for ring in their_x[3:]:
+                ring.step(2)
+            wt_next()
+            own_z.step(4)
+        weight = wbuf[...].reshape(wide, 512)
+        for cut in range(0, 512, 256):
+            proj[:, cut : cut + 256] = dot(nrm[...], weight[:, cut : cut + 256])
         ca, sa = cos_near[...], sin_near[...]
         cosine = ca * cb - sa * sb
         sine = sa * cb + ca * sb
@@ -270,12 +297,44 @@
             swapped = jnp.where(low, pltpu.roll(v, 96, 1), pltpu.roll(v, 32, 1))
             return v * cosine + swapped * sine
 
+        pool = proj[:, 384:512].astype(BF16)
+        pext[16 : 16 + chip, :] = pool.astype(F32)
+        halo[0] = pool[chip - 16 :, :]
+        to_next = post(remote(halo.at[0], halo.at[1], at_chip(1)))
         kbuf[z] = turned(proj[:, 128:256]).astype(BF16)
         vbuf[z] = proj[:, 256:384].T.astype(BF16)
-        kv_ring = Ring(
-            zs, z, at_z, lambda u, s: (kbuf.at[s] if u == 0 else vbuf.at[s]), sems
-        )
-        kv_ring.begin()
+
+        def kv_copy(d, h, u, slot):
+            ref = kbuf.at[slot] if u == 0 else vbuf.at[slot]
+            k = kv_first + (h - 1) * 4 + d * 2 + u
+            return pltpu.make_async_remote_copy(
+                src_ref=ref, dst_ref=ref, send_sem=send_sems.at[k], recv_sem=recv_sems.at[k],
+                device_id=at_z(1 if d == 0 else -1), device_id_type=MESH,
+            )
+
+        kv_first = used[0]
+        used[0] += 2 * zs
+        last = zs // 2
+
+        def kv_slot(d, h):
+            return lax.rem(z + (h if d else -h) + zs, zs)
+
+        def kv_step(h):
+            for u in (0, 1):
+                for d in (0, 1):
+
+                    @pl.when((h < last) | (d == u))
+                    def _():
+                        kv_copy(d, h, u, kv_slot(d, h)).wait_recv()
+
+                        @pl.when((h + 1 < last) | ((h + 1 == last) & (d == u)))
+                        def _():
+                            kv_copy(d, h + 1, u, kv_slot(d, h)).start()
+
+        for u in (0, 1):
+            for d in (0, 1):
+                if last > 1 or d == u:
+                    kv_copy(d, 1, u, z).start()
         queries = (turned(proj[:, 0:128]) * (0.125 * math.log2(math.e))).T.astype(BF16)
         qz[x, 0:64, 0:chip] = queries[0:64]
         qz[x, 64:128, chip : 2 * chip] = queries[64:128]
@@ -285,49 +344,54 @@
         )
         q_ring.begin()
 
-        pool = proj[:, 384:512].astype(BF16)
-        pext[16 : 16 + chip, :] = pool.astype(F32)
-        halo_x[0] = pool[chip - 16 :, :]
-        to_x = post(remote(halo_x.at[0], halo_x.at[1], at_x(1)))
-        wt_ring_z.begin()
-
-        def tile(slot, ch, lt, masked):
-            lanes = pl.ds(lt * LANE_TILE, LANE_TILE)
-            s = dot(kbuf[slot], qz[ch, :, lanes])
-            if masked:
-                offset = (lt * LANE_TILE) % chip
-                visible = lax.broadcasted_iota(jnp.int32, s.shape, 0) <= (
-                    lax.broadcasted_iota(jnp.int32, s.shape, 1) + offset
+        def attend(slot, chunks, masked=False):
+            todo = [(ch, lt) for ch in chunks for lt in range(tiles)]
+
+            def lanes_of(lt):
+                return pl.ds(lt * LANE_TILE, LANE_TILE)
+
+            def scores(ch, lt):
+                return dot(kbuf[slot], qz[ch, :, lanes_of(lt)])
+
+            def add_values(ch, lt, factor, p):
+                lanes = lanes_of(lt)
+                acc[ch, :, lanes] = acc[ch, :, lanes] * factor + dot(vbuf[slot], p)
+
+            ready = [scores(*item) for item in todo[:2]]
+            pending = None
+            for k, (ch, lt) in enumerate(todo):
+                if k + 2 < len(todo):
+                    ready.append(scores(*todo[k + 2]))
+                s = ready.pop(0)
+                lanes = lanes_of(lt)
+                if masked:
+                    offset = (lt * LANE_TILE) % chip
+                    visible = lax.broadcasted_iota(jnp.int32, s.shape, 0) <= (
+                        lax.broadcasted_iota(jnp.int32, s.shape, 1) + offset
+                    )
+                    s = jnp.where(visible, s, low_score)
+                before = mbuf[ch, 0:1, lanes]
+                now = jnp.maximum(before, jnp.max(s, axis=0, keepdims=True))
+                p = jnp.exp2(s - now)
+                factor = jnp.exp2(before - now)
+                mbuf[ch, 0:1, lanes] = now
+                lbuf[ch, 0:1, lanes] = lbuf[ch, 0:1, lanes] * factor + jnp.sum(
+                    p, axis=0, keepdims=True
                 )
-                s = jnp.where(visible, s, low_score)
-            before = mbuf[ch, 0:1, lanes]
-            now = jnp.maximum(before, jnp.max(s, axis=0, keepdims=True))
-            p = jnp.exp2(s - now)
-            factor = jnp.exp2(before - now)
-            mbuf[ch, 0:1, lanes] = now
-            lbuf[ch, 0:1, lanes] = lbuf[ch, 0:1, lanes] * factor + jnp.sum(
-                p, axis=0, keepdims=True
-            )
-            acc[ch, :, lanes] = acc[ch, :, lanes] * factor + dot(vbuf[slot], p.astype(BF16))
-
-        def attend(slot, start):
-            def chunk(ch, carry):
-                for lt in range(tiles):
-                    tile(slot, ch, lt, False)
-                return carry
-
-            lax.fori_loop(start, xs, chunk, 0)
-
-        for lt in range(tiles):
-            tile(z, x, lt, True)
-
-        to_x.wait_recv()
-        to_z = post(remote(halo_x.at[1], halo_z, at_z(1)))
-        for h in range(1, xs // 2 + 1):
-            q_ring.step(h)
-        to_z.wait_recv()
-        from_x, from_z = halo_x[1].astype(F32), halo_z[...].astype(F32)
-        prior = jnp.where(x == 0, from_z, from_x)
+                if pending is not None:
+                    add_values(*pending)
+                pending = (ch, lt, factor, p.astype(BF16))
+            add_values(*pending)
+
+        attend(z, [x], True)
+        q_ring.step(1)
+        wt_next()
+        q_ring.step(2)
+        lax.fori_loop(x + 1, xs, lambda ch, carry: (attend(z, [ch]), carry)[1], 0)
+        wt_next()
+        wt_ring_x.begin()
+        to_next.wait_recv()
+        prior = halo[1].astype(F32)
         pext[0:16, :] = jnp.where(place == 0, 0.0, prior)
         window = jnp.left_shift(2, lax.rem(head, 4))
         whole = pext[...]
@@ -345,36 +409,45 @@
         pooled = (dot(window_mean, gw[head]) * pscale[pl.ds(head, 1), :]).astype(BF16)
         abuf[0, :, 128:256] = pooled[0:tok]
         abuf[1, :, 128:256] = pooled[tok:]
-        attend(z, x + 1)
-
-        for h in range(1, zs // 2 + 1):
-            kv_ring.step(h)
-            wt_ring_z.step(h)
-            if h == zs // 2:
-                wt_ring_x.begin()
-            up, down = kv_ring.slot(0, h), kv_ring.slot(1, h)
-
-            @pl.when(up < z)
+        wt_slots = [x, *(wt_ring_x.slot(d, h) for h in range(1, xs // 2) for d in (0, 1))]
+        wt_slots.append(wt_ring_x.slot(0, xs // 2))
+        wt_shared = [
+            remote(wt.at[:, s, core], wt.at[:, s, core], at_partner()) for s in wt_slots
+        ]
+        sent.extend(wt_shared)
+        wt_shared[0].start()
+
+        def wt_step(h):
+            wt_ring_x.step(h)
+            for copy in wt_shared[1:3] if h == 1 else wt_shared[3:]:
+                copy.start()
+
+        def arrival(k, carry):
+            h, d = k // 2 + 1, lax.rem(k, 2)
+
+            @pl.when(d == 0)
             def _():
-                attend(up, 0)
-
-            if h < zs // 2:
-
-                @pl.when(down < z)
-                def _():
-                    attend(down, 0)
-
-        wt_shared = [
-            post(remote(wt.at[:, x, core], wt.at[:, x, core], at_partner()))
-        ]
-        for h in range(1, xs // 2 + 1):
-            wt_ring_x.step(h)
-            for d in (0, 1):
-                if h < xs // 2 or d == 0:
-                    s = wt_ring_x.slot(d, h)
-                    wt_shared.append(
-                        post(remote(wt.at[:, s, core], wt.at[:, s, core], at_partner()))
-                    )
+                kv_step(h)
+
+            if zs > 2:
+                for hop in range(1, xs // 2 + 1):
+
+                    @pl.when(k == 2 * hop)
+                    def _():
+                        wt_step(hop)
+
+            slot = lax.rem(z + jnp.where(d == 0, -h, h) + zs, zs)
+
+            @pl.when(slot < z)
+            def _():
+                attend(slot, range(xs))
+
+            return carry
+
+        lax.fori_loop(0, zs - 1, arrival, 0)
+        if zs == 2:
+            wt_step(1)
+            wt_step(2)
 
         def share(ch, m):
             lanes = pl.ds(m * chip, chip)
@@ -451,10 +524,8 @@
         for copy in wt_shared:
             copy.wait_recv()
 
-        own_rows = abuf[core]
-        their_rows = abuf[2]
-        rows_0 = jnp.where(core == 0, own_rows, their_rows)
-        rows_1 = jnp.where(core == 0, their_rows, own_rows)
+        rows_0 = jnp.where(core == 0, abuf[core], abuf[2])
+        rows_1 = jnp.where(core == 0, abuf[2], abuf[core])
         per_z = wide // zs
         for s in range(zs):
             weight = wt[s].reshape(per_z, 512)
@@ -501,8 +572,13 @@
 
         for copy in sent:
             copy.wait_send()
-        for ring in (tok_ring, w_ring_x, w_ring_z, wt_ring_x, wt_ring_z, kv_ring, q_ring):
+        for ring in (tok_ring, own_x, own_z, their_z, *their_x, wt_ring_x, wt_ring_z, q_ring):
             ring.finish()
+        for h in range(1, last + 1):
+            for d in (0, 1):
+                for u in (0, 1):
+                    if h < last or d == u:
+                        kv_copy(d, h, u, kv_slot(d, h - 1)).wait_send()
 
     return kernel
 
@@ -527,11 +603,11 @@
         args = (
             tokens, norm_gain.reshape(1, wide), query_one, key_one, query_two, key_two,
             value_weight, pool_weight, lambda_head, head_gain.reshape(1, 128), group_weight,
-            pool_scale.reshape(-1, 128), out_attn, out_pool, *tables,
+            pool_scale.reshape(-1, 128), out_attn.T, out_pool.T, *tables,
         )
         specs = [vmem] * len(args)
         specs[8] = smem
-        semaphores = 128
+        semaphores = 192
         return pl.pallas_call(
             make_kernel(zs, xs, ys, tok, wide),
             out_shape=jax.ShapeDtypeStruct((quarter, wide), BF16),
@@ -542,7 +618,7 @@
                 pltpu.VMEM((zs, xs, 2 * rows, 512), BF16),
                 pltpu.VMEM((zs, xs, 2, rows, 512), BF16),
                 pltpu.VMEM((2, ys, tok, part), BF16),
-                pltpu.VMEM((max(zs, ys), chip, wide // max(zs, ys)), BF16),
+                pltpu.VMEM((chip, wide), BF16),
                 pltpu.VMEM((chip, 512), F32),
                 pltpu.VMEM((zs, chip, 128), BF16),
                 pltpu.VMEM((zs, 128, chip), BF16),
@@ -552,7 +628,6 @@
                 pltpu.VMEM((xs, 8, 2 * chip), F32),
                 pltpu.VMEM((16 + chip, 128), F32),
                 pltpu.VMEM((2, 16, 128), BF16),
-                pltpu.VMEM((16, 128), BF16),
                 pltpu.VMEM((2, 128, chip), BF16),
                 pltpu.VMEM((2, 8, chip), F32),
                 pltpu.VMEM((2, 128, chip), BF16),

time: 135 us -> 97.1 us (0.72)
  the two profiles are of different devices: /device:TPU:225 before, /device:TPU:1 now
where the time goes in v2:
time: 97.1 us; the launch traced here: 97 us
  Pallas kernels  95.3 us (98%)
  local copies, waits for them, and re-layouts  1.67 us (2%)
    pallas_call x1, Pallas kernels, body(): pl.pallas_call(make_kernel(zs, xs, ys, tok, wide), out_shape=jax.ShapeDty...  95.3 us

profile of v2, /device:TPU:1, one launch (start us, length us, event | category | flops | bytes accessed | tf_op | source)
XLA Modules:
  0.0 97.0 jit_solution(6049528341929262088)
XLA Ops:
  0.0 95.3 %mixer.1 = bf16[64,2048]{1,0:T(8,128)(2,1)} custom-call(bf16[256,512]{1,0:T(8,128)(2,1)} %tokens.1, f32[1,2048]{1,0:T(1,128)} %bitcast.7, bf16[32,128]{1,0:T(8,128)(2,1)} %q1.1, bf16[32,128]{1,0:T(8,128)(2,1)} %k1.1, bf16[32,128]{1,0:T(8,128)(2,1)} %q2.1, bf16[32,128]{1,0:T(8,128)(2,1)} %k2.1, bf16[32,256]{1,0:T(8,128)(2,1)} %vw.1, bf16[32,256]{1,0:T(8,128)(2,1)} %pw.1, ...), custom_call_target="tpu_custom_call" | custom-call | tf_op jit(solution)/shard_map/mixer/pallas_call | solution.py:611
  95.3 1.7 %copy.20 = bf16[64,2048]{1,0:T(8,128)(2,1)} copy(bf16[64,2048]{1,0:T(8,128)(2,1)} %mixer.1) | data formatting | bytes 524288

commit v3 on v2

--- a/solution.py
+++ b/solution.py
@@ -14,6 +14,8 @@
 Z_SIZE = 8
 X_SIZE = 4
 LANE_TILE = 256
+SEND_SEMAPHORES = 32
+RECV_SEMAPHORES = 128
 
 rope_base = 500000.0
 head_scale = 0.8
@@ -37,54 +39,51 @@
 
 
 class Ring:
-    def __init__(self, n, me, device, unit, sems):
-        self.n, self.me, self.device, self.unit = n, me, device, unit
-        self.sems = {}
-        for h in range(1, n // 2 + 1):
-            for d in (0, 1):
-                for u in (0, 1):
-                    if self.has(d, h, u):
-                        self.sems[d, h, u] = sems()
-
-    def has(self, d, h, u):
-        return h < self.n // 2 or (h == self.n // 2 and d == u)
+    def __init__(self, n, me, device, unit, send_sem, recv_sem, whole=False):
+        self.n, self.me, self.device, self.unit, self.whole = n, me, device, unit, whole
+        self.send_sem = send_sem
+        self.recv = {(d, h, p): recv_sem() for h in range(1, n // 2 + 1) for d in (0, 1) for p in self.parts(d, h)}
+
+    def parts(self, d, h):
+        if h == self.n // 2:
+            return (d,)
+        return (None,) if self.whole else (0, 1)
 
     def slot(self, d, h):
-        sign = 1 if d == 0 else -1
-        return lax.rem(self.me - sign * h + self.n, self.n)
-
-    def copy(self, d, h, u, slot):
-        ref = self.unit(u, slot)
-        send_sem, recv_sem = self.sems[d, h, u]
+        return lax.rem(self.me + (h if d else -h) + self.n, self.n)
+
+    def copy(self, d, h, p, slot):
+        ref = self.unit(p, slot)
         return pltpu.make_async_remote_copy(
             src_ref=ref,
             dst_ref=ref,
-            send_sem=send_sem,
-            recv_sem=recv_sem,
-            device_id=self.device(1 if d == 0 else -1),
+            send_sem=self.send_sem,
+            recv_sem=self.recv[d, h, p],
+            device_id=self.device(-1 if d else 1),
             device_id_type=MESH,
         )
 
-    def send(self, d, h, u):
-        self.copy(d, h, u, self.slot(d, h - 1)).start()
-
-    def begin(self, units=(0, 1)):
-        for u in units:
+    def send(self, d, h, p):
+        self.copy(d, h, p, self.slot(d, h - 1)).start()
+
+    def begin(self):
+        for d in (0, 1):
+            for p in self.parts(d, 1):
+                self.send(d, 1, p)
+
+    def step(self, h):
+        units = (None,) if self.whole else (0, 1)
+        for p in units if h < self.n // 2 else (0, 1):
             for d in (0, 1):
-                if self.has(d, 1, u):
-                    self.send(d, 1, u)
-
-    def step(self, h):
-        for u in (0, 1):
-            for d in (0, 1):
-                if self.has(d, h, u):
-                    self.copy(d, h, u, self.slot(d, h)).wait_recv()
-                    if (d, h + 1, u) in self.sems:
-                        self.send(d, h + 1, u)
-
-    def finish(self):
-        for d, h, u in self.sems:
-            self.copy(d, h, u, self.slot(d, h - 1)).wait_send()
+                if p in self.parts(d, h):
+                    self.copy(d, h, p, self.slot(d, h)).wait_recv()
+                    if h + 1 < self.n // 2:
+                        self.send(d, h + 1, p)
+                    elif h + 1 == self.n // 2 and p in (None, d):
+                        self.send(d, h + 1, d)
+
+    def sent_bytes(self, slot_bytes):
+        return sum(slot_bytes if p is None else slot_bytes // 2 for _, _, p in self.recv)
 
 
 def dot(a, b, dims=((1,), (0,))):
@@ -130,26 +129,29 @@
         def at_partner():
             return {"sp": place * 2 + other, "tp": y}
 
-        used = [0]
-
-        def sems():
+        used, used_send = [0], [0]
+
+        def recv_sem(count=1):
             k = used[0]
-            used[0] += 1
-            return send_sems.at[k], recv_sems.at[k]
-
-        def remote(src, dst, device):
-            send_sem, recv_sem = sems()
+            used[0] += count
+            return recv_sems.at[k]
+
+        def send_sem():
+            k = used_send[0]
+            used_send[0] += 1
+            return send_sems.at[k]
+
+        def remote(src, dst, device, sem):
             return pltpu.make_async_remote_copy(
-                src_ref=src, dst_ref=dst, send_sem=send_sem, recv_sem=recv_sem,
+                src_ref=src, dst_ref=dst, send_sem=sem, recv_sem=recv_sem(),
                 device_id=device, device_id_type=MESH,
             )
 
-        sent = []
-
-        def post(copy):
-            copy.start()
-            sent.append(copy)
-            return copy
+        def drain(sem, size):
+            rows_sent = wbuf.reshape(zs * xs * 2 * rows, 512).at[pl.ds(0, size // 1024), :]
+            pltpu.make_async_copy(rows_sent, rows_sent, sem).wait()
+
+        rows = q1.shape[0]
 
         def by_head(h):
             a, b = h * 64, h * 64 + 64
@@ -158,11 +160,9 @@
                 [q1[:, a:b], q2[:, a:b], k1[:, a:b], k2[:, a:b], vw[:, c:d], pw[:, c:d]], axis=1
             )
 
-        rows = q1.shape[0]
         first, second = by_head(0), by_head(1)
         mine = core == 0
         own_rows = pl.ds(core * rows, rows)
-        their_rows = pl.ds(other * rows, rows)
         wbuf[z, x, own_rows, :] = jnp.where(mine, first, second)
         wsend[...] = jnp.where(mine, second, first)
         tokbuf[core, y] = tokens[...]
@@ -182,80 +182,116 @@
             pl.semaphore_signal(barrier, inc=1, device_id=device, device_id_type=MESH)
         pl.semaphore_wait(barrier, len(neighbours))
 
-        w_swap = post(remote(wsend, wbuf.at[z, x, own_rows, :], at_partner()))
+        misc_sem, share_sem, wt_share_sem, mean_sem, sum_sem = (send_sem() for _ in range(5))
+        w_swap = remote(wsend, wbuf.at[z, x, own_rows, :], at_partner(), misc_sem)
+        w_swap.start()
         half = tok // 2
-        strip = rows // 2
+        lead = rows
+        rest = 2 * rows - lead
+        row_bytes = 512 * 2
+        lead_from, rest_from = core * rest, other * lead
+
+        def pieces(first_row, size, p):
+            return pl.ds(first_row, size) if p is None else pl.ds(first_row + p * (size // 2), size // 2)
+
         tok_ring = Ring(
-            ys, y, at_y, lambda u, s: tokbuf.at[core, s, pl.ds(u * half, half), :], sems
-        )
-        own_x = Ring(
-            xs, x, at_x,
-            lambda u, s: wbuf.at[z, s, pl.ds(core * rows + u * strip, strip), :], sems,
-        )
-        own_z = Ring(
-            zs, z, at_z,
-            lambda u, s: wbuf.at[s, pl.ds(u * (xs // 2), xs // 2), own_rows, :], sems,
-        )
-        their_z = Ring(
-            zs, z, at_z,
-            lambda u, s: wbuf.at[s, x, pl.ds(other * rows + u * strip, strip), :], sems,
+            ys, y, at_y, lambda p, s: tokbuf.at[core, s, pl.ds(p * half, half), :],
+            send_sem(), recv_sem,
+        )
+        lead_x = Ring(
+            xs, x, at_x, lambda p, s: wbuf.at[z, s, pieces(lead_from, lead, p), :],
+            send_sem(), recv_sem, True,
+        )
+        lead_z = Ring(
+            zs, z, at_z, lambda p, s: wbuf.at[s, pl.ds(p * (xs // 2), xs // 2), pl.ds(lead_from, lead), :],
+            send_sem(), recv_sem,
+        )
+        rest_z = Ring(
+            zs, z, at_z, lambda p, s: wbuf.at[s, x, pieces(rest_from, rest, p), :],
+            send_sem(), recv_sem, True,
         )
         wt_ring_z = Ring(
-            zs, z, at_z, lambda u, s: wt.at[s, x, core, pl.ds(u * strip, strip), :], sems
-        )
+            zs, z, at_z, lambda p, s: wt.at[s, x, core, pieces(0, rows, p), :],
+            send_sem(), recv_sem, True,
+        )
+
+        def half_z(p):
+            return slice(None) if p is None else pl.ds(p * (zs // 2), zs // 2)
+
         wt_ring_x = Ring(
-            xs, x, at_x, lambda u, s: wt.at[pl.ds(u * (zs // 2), zs // 2), s, core], sems
-        )
-
-        def their_x_ring(slot):
+            xs, x, at_x, lambda p, s: wt.at[half_z(p), s, core], send_sem(), recv_sem, True
+        )
+
+        def rest_x_ring(slot):
             ring = Ring(
-                xs, x, at_x,
-                lambda u, s: wbuf.at[slot, s, pl.ds(other * rows + u * strip, strip), :], sems,
+                xs, x, at_x, lambda p, s: wbuf.at[slot, s, pieces(rest_from, rest, p), :],
+                send_sem(), recv_sem, True,
             )
             ring.begin()
             return ring
 
-        own_x.begin()
+        lead_x.begin()
         tok_ring.begin()
+        shared = []
 
         def share_tokens(s):
-            return post(remote(tokbuf.at[core, s], tokbuf.at[core, s], at_partner()))
-
-        shared = [share_tokens(y)]
+            copy = remote(tokbuf.at[core, s], tokbuf.at[core, s], at_partner(), share_sem)
+            copy.start()
+            shared.append(copy)
+
+        share_tokens(y)
         cb, sb = cos_far[pl.ds(place, 1), :], sin_far[pl.ds(place, 1), :]
         w_swap.wait_recv()
-        their_z.begin()
-        their_x = [their_x_ring(z)]
-
-        def their_step(h):
-            their_z.step(h)
-            their_x.append(their_x_ring(their_z.slot(0, h)))
-            if h < zs // 2:
-                their_x.append(their_x_ring(their_z.slot(1, h)))
+        rest_z.begin()
+        rest_x = [rest_x_ring(z)]
+
+        def rest_step(h):
+            if h <= zs // 2:
+                rest_z.step(h)
+                rest_x.append(rest_x_ring(rest_z.slot(0, h)))
+                if h < zs // 2:
+                    rest_x.append(rest_x_ring(rest_z.slot(1, h)))
+
+        relayed = [0]
+
+        def relay(count=zs):
+            while relayed[0] < min(count, len(rest_x)):
+                rest_x[relayed[0]].step(1)
+                relayed[0] += 1
+
+        def lead_step(h):
+            if h <= zs // 2:
+                lead_z.step(h)
 
         def tok_step(h):
             tok_ring.step(h)
-            shared.append(share_tokens(tok_ring.slot(0, h)))
+            share_tokens(tok_ring.slot(0, h))
             if h < ys // 2:
-                shared.append(share_tokens(tok_ring.slot(1, h)))
-
-        own_x.step(1)
-        their_step(1)
-        own_x.step(2)
-        own_z.begin()
-        if zs > 2:
-            their_step(2)
-            their_step(3)
+                share_tokens(tok_ring.slot(1, h))
+
+        wt_hops = list(range(1, zs // 2 + 1))
+
+        def wt_next():
+            if wt_hops:
+                wt_ring_z.step(wt_hops.pop(0))
+
+        lead_x.step(1)
+        rest_step(1)
+        lead_x.step(2)
+        lead_z.begin()
+        relay(1)
+        rest_step(2)
         tok_step(1)
-        for ring in their_x[:3]:
-            ring.step(1)
-        if zs > 2:
-            their_step(4)
-        own_z.step(1)
+        rest_step(3)
+        lead_step(1)
+        relay(3)
+        rest_step(4)
+        lead_step(2)
+        relay(5)
+        tok_step(2)
+        lead_step(3)
+        relay(7)
         wt_ring_z.begin()
-        for ring in their_x[:3]:
-            ring.step(2)
-        tok_step(2)
         for copy in shared:
             copy.wait_recv()
 
@@ -269,22 +305,11 @@
                 block = tokbuf[owner, s].astype(F32) * scale * gain[:, s * part : (s + 1) * part]
                 nrm[owner * tok : (owner + 1) * tok, s * part : (s + 1) * part] = block.astype(BF16)
 
-        wt_hops = list(range(1, zs // 2 + 1))
-
-        def wt_next():
-            if wt_hops:
-                wt_ring_z.step(wt_hops.pop(0))
-
-        if zs > 2:
-            own_z.step(2)
-            for ring in their_x[3:]:
-                ring.step(1)
-            wt_next()
-            own_z.step(3)
-            for ring in their_x[3:]:
-                ring.step(2)
-            wt_next()
-            own_z.step(4)
+        lead_step(4)
+        relay()
+        for ring in rest_x:
+            ring.step(2)
+        wt_next()
         weight = wbuf[...].reshape(wide, 512)
         for cut in range(0, 512, 256):
             proj[:, cut : cut + 256] = dot(nrm[...], weight[:, cut : cut + 256])
@@ -300,7 +325,8 @@
         pool = proj[:, 384:512].astype(BF16)
         pext[16 : 16 + chip, :] = pool.astype(F32)
         halo[0] = pool[chip - 16 :, :]
-        to_next = post(remote(halo.at[0], halo.at[1], at_chip(1)))
+        to_next = remote(halo.at[0], halo.at[1], at_chip(1), send_sem())
+        to_next.start()
         kbuf[z] = turned(proj[:, 128:256]).astype(BF16)
         vbuf[z] = proj[:, 256:384].T.astype(BF16)
 
@@ -308,12 +334,13 @@
             ref = kbuf.at[slot] if u == 0 else vbuf.at[slot]
             k = kv_first + (h - 1) * 4 + d * 2 + u
             return pltpu.make_async_remote_copy(
-                src_ref=ref, dst_ref=ref, send_sem=send_sems.at[k], recv_sem=recv_sems.at[k],
+                src_ref=ref, dst_ref=ref, send_sem=kv_send, recv_sem=recv_sems.at[k],
                 device_id=at_z(1 if d == 0 else -1), device_id_type=MESH,
             )
 
         kv_first = used[0]
-        used[0] += 2 * zs
+        recv_sem(2 * zs)
+        kv_send = send_sem()
         last = zs // 2
 
         def kv_slot(d, h):
@@ -340,7 +367,8 @@
         qz[x, 64:128, chip : 2 * chip] = queries[64:128]
         q_ring = Ring(
             xs, x, at_x,
-            lambda u, s: qz.at[s, pl.ds(64 * u, 64), pl.ds(chip * u, chip)], sems,
+            lambda p, s: qz.at[s, pl.ds(64 * p, 64), pl.ds(chip * p, chip)],
+            send_sem(), recv_sem,
         )
         q_ring.begin()
 
@@ -384,11 +412,29 @@
             add_values(*pending)
 
         attend(z, [x], True)
+        wt_next()
+        ahead = lax.rem(x + 1, xs)
+        behind = lax.rem(x + xs - 1, xs)
+        across = lax.rem(x + 2, xs)
         q_ring.step(1)
         wt_next()
-        q_ring.step(2)
-        lax.fori_loop(x + 1, xs, lambda ch, carry: (attend(z, [ch]), carry)[1], 0)
-        wt_next()
+
+        def own_block(k, carry):
+            ch = jnp.where(k == 0, ahead, jnp.where(k == 1, behind, across))
+
+            @pl.when(k == 2)
+            def _():
+                q_ring.step(2)
+
+            @pl.when(ch > x)
+            def _():
+                attend(z, [ch])
+
+            return carry
+
+        lax.fori_loop(0, 3, own_block, 0)
+        while wt_hops:
+            wt_next()
         wt_ring_x.begin()
         to_next.wait_recv()
         prior = halo[1].astype(F32)
@@ -409,18 +455,13 @@
         pooled = (dot(window_mean, gw[head]) * pscale[pl.ds(head, 1), :]).astype(BF16)
         abuf[0, :, 128:256] = pooled[0:tok]
         abuf[1, :, 128:256] = pooled[tok:]
-        wt_slots = [x, *(wt_ring_x.slot(d, h) for h in range(1, xs // 2) for d in (0, 1))]
-        wt_slots.append(wt_ring_x.slot(0, xs // 2))
+        wt_slots = [x, behind, ahead, across]
         wt_shared = [
-            remote(wt.at[:, s, core], wt.at[:, s, core], at_partner()) for s in wt_slots
+            remote(wt.at[:, s, core], wt.at[:, s, core], at_partner(), wt_share_sem)
+            for s in wt_slots
         ]
-        sent.extend(wt_shared)
+
         wt_shared[0].start()
-
-        def wt_step(h):
-            wt_ring_x.step(h)
-            for copy in wt_shared[1:3] if h == 1 else wt_shared[3:]:
-                copy.start()
 
         def arrival(k, carry):
             h, d = k // 2 + 1, lax.rem(k, 2)
@@ -429,25 +470,31 @@
             def _():
                 kv_step(h)
 
-            if zs > 2:
-                for hop in range(1, xs // 2 + 1):
-
-                    @pl.when(k == 2 * hop)
-                    def _():
-                        wt_step(hop)
+            @pl.when(k == 4)
+            def _():
+                wt_ring_x.step(1)
+                for copy in wt_shared[1:3]:
+                    copy.start()
 
             slot = lax.rem(z + jnp.where(d == 0, -h, h) + zs, zs)
 
             @pl.when(slot < z)
             def _():
-                attend(slot, range(xs))
+                attend(slot, [across, ahead, behind, x])
 
             return carry
 
-        lax.fori_loop(0, zs - 1, arrival, 0)
+        lax.fori_loop(0, zs - 2, arrival, 0)
         if zs == 2:
-            wt_step(1)
-            wt_step(2)
+            wt_ring_x.step(1)
+            for copy in wt_shared[1:3]:
+                copy.start()
+        kv_step(last)
+        farthest = kv_slot(0, last)
+
+        @pl.when(farthest < z)
+        def _():
+            attend(farthest, [across])
 
         def share(ch, m):
             lanes = pl.ds(m * chip, chip)
@@ -457,6 +504,32 @@
             weight = jnp.where(some, mbuf[ch, 0:1, lanes] + jnp.log2(safe), low_score)
             return acc[ch, :, lanes] * (1.0 / safe), weight
 
+        def put(pair, o_ref, e_ref):
+            o_ref[...] = pair[0].astype(BF16)
+            e_ref[...] = pair[1]
+
+        def send_pair(o_src, e_src, o_dst, e_dst, device):
+            pair = (remote(o_src, o_dst, device, mean_sem), remote(e_src, e_dst, device, send_sem()))
+            for copy in pair:
+                copy.start()
+            stat_copies.append(pair[1])
+            return pair
+
+        stat_copies = []
+        sides = ((ahead, at_x(1)), (behind, at_x(-1)))
+        first_hop = []
+        for m in (0, 1):
+            put(share(across, m), o1s.at[m], e1s.at[m])
+            first_hop.append(
+                send_pair(o1s.at[m], e1s.at[m], o1r.at[m], e1r.at[m], sides[m][1])
+            )
+
+        @pl.when(farthest < z)
+        def _():
+            attend(farthest, [ahead, behind, x])
+
+        wt_ring_x.step(2)
+        wt_shared[3].start()
         def joined(*shares):
             top = shares[0][1]
             for _, weight in shares[1:]:
@@ -466,26 +539,9 @@
             value = sum(o * f for (o, _), f in zip(shares, factors)) * (1.0 / total)
             return value, top + jnp.log2(total)
 
-        def put(pair, o_ref, e_ref):
-            o_ref[...] = pair[0].astype(BF16)
-            e_ref[...] = jnp.broadcast_to(pair[1], e_ref.shape)
-
-        def send_pair(o_src, e_src, o_dst, e_dst, device):
-            return post(remote(o_src, o_dst, device)), post(remote(e_src, e_dst, device))
-
         def get(o_ref, e_ref):
-            return o_ref[...].astype(F32), e_ref[0:1, :]
-
-        ahead = lax.rem(x + 1, xs)
-        behind = lax.rem(x + xs - 1, xs)
-        across = lax.rem(x + 2, xs)
-        sides = ((ahead, at_x(1)), (behind, at_x(-1)))
-        first_hop = []
-        for m in (0, 1):
-            put(share(across, m), o1s.at[m], e1s.at[m])
-            first_hop.append(
-                send_pair(o1s.at[m], e1s.at[m], o1r.at[m], e1r.at[m], sides[m][1])
-            )
+            return o_ref[...].astype(F32), e_ref[...]
+
         second_hop = []
         for m in (0, 1):
             chunk, device = sides[m]
@@ -519,7 +575,8 @@
 
         abuf[0, :, 0:128] = attn[0:tok]
         abuf[1, :, 0:128] = attn[tok:]
-        swap = post(remote(abuf.at[other], abuf.at[2], at_partner()))
+        swap = remote(abuf.at[other], abuf.at[2], at_partner(), send_sem())
+        swap.start()
         swap.wait_recv()
         for copy in wt_shared:
             copy.wait_recv()
@@ -545,22 +602,24 @@
             return pl.ds(target * quarter + m * y_half, y_half)
 
         y_first, y_second = [], []
+
+        def send_sum(src, dst, device, group):
+            copy = remote(src, dst, device, sum_sem)
+            copy.start()
+            group.append(copy)
+
         for m in (0, 1):
-            y_first.append(
-                post(remote(ysum.at[rows_of(y_across, m), :], y1r.at[m], y_sides[m][1]))
-            )
+            send_sum(ysum.at[rows_of(y_across, m), :], y1r.at[m], y_sides[m][1], y_first)
         for m in (0, 1):
             target, device = y_sides[m]
-            y_second.append(
-                post(remote(ysum.at[rows_of(target, 1 - m), :], y2r.at[m, 1 - m], device))
-            )
+            send_sum(ysum.at[rows_of(target, 1 - m), :], y2r.at[m, 1 - m], device, y_second)
         for m in (0, 1):
             target, device = y_sides[m]
             y_first[m].wait_recv()
             y2s[m] = (
                 ysum[rows_of(target, m), :].astype(F32) + y1r[m].astype(F32)
             ).astype(BF16)
-            y_second.append(post(remote(y2s.at[m], y2r.at[m, m], device)))
+            send_sum(y2s.at[m], y2r.at[m, m], device, y_second)
         for copy in y_second:
             copy.wait_recv()
         for m in (0, 1):
@@ -570,15 +629,26 @@
                 + y2r[1, m].astype(F32)
             ).astype(BF16)
 
-        for copy in sent:
+        slot_bytes = (
+            (tok_ring, tok * part * 2),
+            (lead_x, lead * row_bytes),
+            (lead_z, xs * lead * row_bytes),
+            (rest_z, rest * row_bytes),
+            *((ring, rest * row_bytes) for ring in rest_x),
+            (wt_ring_z, rows * row_bytes),
+            (wt_ring_x, zs * rows * row_bytes),
+            (q_ring, chip * 256),
+        )
+        for ring, size in slot_bytes:
+            drain(ring.send_sem, ring.sent_bytes(size))
+        drain(kv_send, (zs - 1) * chip * 512)
+        drain(share_sem, ys * tok * part * 2)
+        drain(wt_share_sem, zs * xs * rows * row_bytes)
+        drain(mean_sem, 6 * chip * 256)
+        drain(sum_sem, 6 * (quarter // 2) * wide * 2)
+        for copy in (w_swap, to_next, swap, *stat_copies):
             copy.wait_send()
-        for ring in (tok_ring, own_x, own_z, their_z, *their_x, wt_ring_x, wt_ring_z, q_ring):
-            ring.finish()
-        for h in range(1, last + 1):
-            for d in (0, 1):
-                for u in (0, 1):
-                    if h < last or d == u:
-                        kv_copy(d, h, u, kv_slot(d, h - 1)).wait_send()
+        assert used[0] <= RECV_SEMAPHORES and used_send[0] <= SEND_SEMAPHORES, (used, used_send)
 
     return kernel
 
@@ -607,7 +677,6 @@
         )
         specs = [vmem] * len(args)
         specs[8] = smem
-        semaphores = 192
         return pl.pallas_call(
             make_kernel(zs, xs, ys, tok, wide),
             out_shape=jax.ShapeDtypeStruct((quarter, wide), BF16),
@@ -629,20 +698,20 @@
                 pltpu.VMEM((16 + chip, 128), F32),
                 pltpu.VMEM((2, 16, 128), BF16),
                 pltpu.VMEM((2, 128, chip), BF16),
-                pltpu.VMEM((2, 8, chip), F32),
+                pltpu.VMEM((2, 1, chip), F32),
                 pltpu.VMEM((2, 128, chip), BF16),
-                pltpu.VMEM((2, 8, chip), F32),
+                pltpu.VMEM((2, 1, chip), F32),
                 pltpu.VMEM((2, 2, 128, chip), BF16),
-                pltpu.VMEM((2, 2, 8, chip), F32),
+                pltpu.VMEM((2, 2, 1, chip), F32),
                 pltpu.VMEM((2, 2, 128, chip), BF16),
-                pltpu.VMEM((2, 2, 8, chip), F32),
+                pltpu.VMEM((2, 2, 1, chip), F32),
                 pltpu.VMEM((3, tok, 256), BF16),
                 pltpu.VMEM((tok, wide), BF16),
                 pltpu.VMEM((2, quarter // 2, wide), BF16),
                 pltpu.VMEM((2, quarter // 2, wide), BF16),
                 pltpu.VMEM((2, 2, quarter // 2, wide), BF16),
-                pltpu.SemaphoreType.DMA((semaphores,)),
-                pltpu.SemaphoreType.DMA((semaphores,)),
+                pltpu.SemaphoreType.DMA((SEND_SEMAPHORES,)),
+                pltpu.SemaphoreType.DMA((RECV_SEMAPHORES,)),
             ],
             compiler_params=pltpu.CompilerParams(
                 collective_id=0, has_side_effects=True, vmem_limit_bytes=60 * 1024 * 1024

time: 97.1 us -> 92.9 us (0.957)
  Pallas kernels: 95.3 us -> 91.1 us
    pallas_call x1, Pallas kernels: 95.3 us -> 91.1 us  [body(): pl.pallas_call(make_kernel(zs, xs, ys, tok, wide), out_shape=jax.ShapeDty...]
where the time goes in v3:
time: 92.9 us; the launch traced here: 92.8 us
  Pallas kernels  91.1 us (98%)
  local copies, waits for them, and re-layouts  1.67 us (2%)
    pallas_call x1, Pallas kernels, body(): pl.pallas_call(make_kernel(zs, xs, ys, tok, wide), out_shape=jax.ShapeDty...  91.1 us

profile of v3, /device:TPU:1, one launch (start us, length us, event | category | flops | bytes accessed | tf_op | source)
XLA Modules:
  0.0 92.8 jit_solution(9565809396909864897)
XLA Ops:
  0.0 91.1 %mixer.1 = bf16[64,2048]{1,0:T(8,128)(2,1)} custom-call(bf16[256,512]{1,0:T(8,128)(2,1)} %tokens.1, f32[1,2048]{1,0:T(1,128)} %bitcast.7, bf16[32,128]{1,0:T(8,128)(2,1)} %q1.1, bf16[32,128]{1,0:T(8,128)(2,1)} %k1.1, bf16[32,128]{1,0:T(8,128)(2,1)} %q2.1, bf16[32,128]{1,0:T(8,128)(2,1)} %k2.1, bf16[32,256]{1,0:T(8,128)(2,1)} %vw.1, bf16[32,256]{1,0:T(8,128)(2,1)} %pw.1, ...), custom_call_target="tpu_custom_call" | custom-call | tf_op jit(solution)/shard_map/mixer/pallas_call | solution.py:680
  91.2 1.7 %copy.20 = bf16[64,2048]{1,0:T(8,128)(2,1)} copy(bf16[64,2048]{1,0:T(8,128)(2,1)} %mixer.1) | data formatting | bytes 524288

commit v4 on v3

--- a/solution.py
+++ b/solution.py
@@ -279,19 +279,23 @@
         rest_step(1)
         lead_x.step(2)
         lead_z.begin()
+        wt_ring_z.begin()
         relay(1)
         rest_step(2)
         tok_step(1)
+        relay(3)
+        wt_next()
+        lead_step(1)
         rest_step(3)
-        lead_step(1)
-        relay(3)
+        wt_next()
         rest_step(4)
+        relay(5)
         lead_step(2)
-        relay(5)
+        relay(7)
+        wt_next()
         tok_step(2)
+        relay(8)
         lead_step(3)
-        relay(7)
-        wt_ring_z.begin()
         for copy in shared:
             copy.wait_recv()
 
@@ -306,7 +310,6 @@
                 nrm[owner * tok : (owner + 1) * tok, s * part : (s + 1) * part] = block.astype(BF16)
 
         lead_step(4)
-        relay()
         for ring in rest_x:
             ring.step(2)
         wt_next()
@@ -412,12 +415,10 @@
             add_values(*pending)
 
         attend(z, [x], True)
-        wt_next()
         ahead = lax.rem(x + 1, xs)
         behind = lax.rem(x + xs - 1, xs)
         across = lax.rem(x + 2, xs)
         q_ring.step(1)
-        wt_next()
 
         def own_block(k, carry):
             ch = jnp.where(k == 0, ahead, jnp.where(k == 1, behind, across))
@@ -433,8 +434,6 @@
             return carry
 
         lax.fori_loop(0, 3, own_block, 0)
-        while wt_hops:
-            wt_next()
         wt_ring_x.begin()
         to_next.wait_recv()
         prior = halo[1].astype(F32)

time: 92.9 us -> 90.5 us (0.974)
  Pallas kernels: 91.1 us -> 88.7 us
    pallas_call x1, Pallas kernels: 91.1 us -> 88.7 us  [body(): pl.pallas_call(make_kernel(zs, xs, ys, tok, wide), out_shape=jax.ShapeDty...]
where the time goes in v4:
time: 90.5 us; the launch traced here: 90.4 us
  Pallas kernels  88.7 us (98%)
  local copies, waits for them, and re-layouts  1.67 us (2%)
    pallas_call x1, Pallas kernels, body(): pl.pallas_call(make_kernel(zs, xs, ys, tok, wide), out_shape=jax.ShapeDty...  88.7 us

profile of v4, /device:TPU:1, one launch (start us, length us, event | category | flops | bytes accessed | tf_op | source)
XLA Modules:
  0.0 90.4 jit_solution(9982187254937038251)
XLA Ops:
  0.0 88.7 %mixer.1 = bf16[64,2048]{1,0:T(8,128)(2,1)} custom-call(bf16[256,512]{1,0:T(8,128)(2,1)} %tokens.1, f32[1,2048]{1,0:T(1,128)} %bitcast.7, bf16[32,128]{1,0:T(8,128)(2,1)} %q1.1, bf16[32,128]{1,0:T(8,128)(2,1)} %k1.1, bf16[32,128]{1,0:T(8,128)(2,1)} %q2.1, bf16[32,128]{1,0:T(8,128)(2,1)} %k2.1, bf16[32,256]{1,0:T(8,128)(2,1)} %vw.1, bf16[32,256]{1,0:T(8,128)(2,1)} %pw.1, ...), custom_call_target="tpu_custom_call" | custom-call | tf_op jit(solution)/shard_map/mixer/pallas_call | solution.py:679
  88.7 1.7 %copy.20 = bf16[64,2048]{1,0:T(8,128)(2,1)} copy(bf16[64,2048]{1,0:T(8,128)(2,1)} %mixer.1) | data formatting | bytes 524288
